TPU v7x, 32 devices: a whole 2x2x4 slice. The times are simulated.
32 devices in a mesh: sp: 8 (over z, y), tp: 4 (over x, core).
Axes of the slice: x: 2, y: 2, z: 4, core: 2. Of those that a mesh axis runs over, the one named last changes fastest.
Arguments:
- residual: bfloat16 [8192, 2048], P(('sp', 'tp')), may hold values from -6 to 6
- pool_input: bfloat16 [8192, 1024], P('sp', 'tp'), may hold values from -6 to 6
- doc_ids: int32 [8192], P('sp'), may hold values from 0 to 3, never falling along the last dimension, each value on 1 to 4096 neighbouring positions
- pool_map: bfloat16 [4, 256, 256], P('tp'), may hold values from -0.375 to 0.375
- pool_scale: float32 [1024], P('tp'), may hold values from 0.1 to 1.9
- out_weight: bfloat16 [1024, 2048], replicated, may hold values from -0.1875 to 0.1875
- mix_gain: float32 [2048], replicated, may hold values from 0.1 to 1.9
- mix_shift: float32 [2048], replicated, may hold values from -1.75 to 1.75
- group_router: bfloat16 [2048, 4], replicated, may hold values from -0.125 to 0.125
- expert_router: bfloat16 [2048, 8], replicated, may hold values from -0.125 to 0.125
- expert_gate: bfloat16 [8, 2048, 512], P('sp'), may hold values from -0.375 to 0.375
- expert_up: bfloat16 [8, 2048, 512], P('sp'), may hold values from -0.375 to 0.375
- expert_down: bfloat16 [8, 512, 2048], P('sp'), may hold values from -0.75 to 0.75
- routes: int32 [8192, 2], P(('sp', 'tp')), may hold values from 0 to 7, as said below
- ffn_gain: float32 [2048], replicated, may hold values from 0.1 to 1.9
- ffn_shift: float32 [2048], replicated, may hold values from -1.75 to 1.75
Outputs:
- layer_out: bfloat16 [8192, 2048], P(('sp', 'tp'))
Inputs may be any that keep to these rules, and one draw needn't show every extreme that they name: `doc_ids`: document numbers never fall along the positions; each document has 1 to 4096 positions. `routes`: A token names 2 different experts. In each aligned block of half of one device's 256 rows, 4 experts are named exactly 64 times each and the others not at all.
All inputs are finite; a program needn't handle non-finite values.
Results may differ from a plain program's by a relative error of at most 0.0073.
Values may be sent and summed in bfloat16 or wider, within the bound.
A program may use at most 128 MiB of HBM per device.

v0:
```python
import functools

import jax
import jax.numpy as jnp
from jax import lax
from jax.experimental import pallas as pl
from jax.experimental.pallas import tpu as pltpu
from jax.sharding import PartitionSpec as P

skip_scale = 2.0**0.5
epsilon = 1e-05


def from_behind(block, axis, distance):
    devices = range(lax.axis_size(axis))
    route = [(i - distance, i) for i in devices if i - distance in devices]
    return lax.ppermute(block, axis, route)


def layer_norm(values, norm_gain, norm_shift):
    center = values - jnp.mean(values, axis=-1, keepdims=True)
    spread = jnp.mean(center * center, axis=-1, keepdims=True)
    return center * lax.rsqrt(spread + epsilon) * norm_gain + norm_shift


def route_weights(normed, chosen, group_router, expert_router):
    group_logits = jnp.dot(normed, group_router, preferred_element_type=jnp.float32)
    expert_logits = jnp.dot(normed, expert_router, preferred_element_type=jnp.float32)
    group_count = group_logits.shape[1]
    expert_count = expert_logits.shape[1]
    group_exp = jnp.exp(group_logits)
    group_prob = group_exp / jnp.sum(group_exp, axis=1, keepdims=True)
    expert_ids = jnp.arange(expert_count, dtype=jnp.int32)
    picked = jnp.sum(
        jnp.where(chosen[:, :, None] == expert_ids[None, None, :], expert_logits[:, None, :], 0.0),
        axis=2,
    )
    picked_exp = jnp.exp(picked)
    pair_share = picked_exp / jnp.sum(picked_exp, axis=1, keepdims=True)
    group_of = chosen // (expert_count // group_count)
    group_ids = jnp.arange(group_count, dtype=jnp.int32)
    group_share = jnp.sum(
        jnp.where(group_of[:, :, None] == group_ids[None, None, :], group_prob[:, None, :], 0.0),
        axis=2,
    )
    return group_share * pair_share


def expert_ffn(arrived, expert_gate, expert_up, expert_down):
    sources, slot_count, width = arrived.shape
    gathered = arrived.reshape(sources * slot_count, width)
    gate_out = jnp.dot(gathered, expert_gate[0], preferred_element_type=jnp.float32)
    up_out = jnp.dot(gathered, expert_up[0], preferred_element_type=jnp.float32)
    hidden = (jax.nn.silu(gate_out) * up_out).astype(jnp.bfloat16)
    result = jnp.dot(hidden, expert_down[0], preferred_element_type=jnp.float32).astype(
        jnp.bfloat16
    )
    return result.reshape(sources, slot_count, width)


def fill_slots(normed, chosen, capacity, expert_count):
    flat_routes = chosen.reshape(-1)
    entry_count = flat_routes.shape[0]
    onehot = (flat_routes[:, None] == jnp.arange(expert_count, dtype=jnp.int32)[None, :]).astype(
        jnp.int32
    )
    slot_rank = jnp.sum((jnp.cumsum(onehot, axis=0) - onehot) * onehot, axis=1)
    slot_index = flat_routes * capacity + slot_rank
    token_ids = jnp.arange(entry_count, dtype=jnp.int32) // chosen.shape[1]
    source_row = (
        jnp.full((expert_count * capacity,), normed.shape[0], jnp.int32)
        .at[slot_index]
        .set(token_ids)
    )
    padded = jnp.concatenate([normed, jnp.zeros((1, normed.shape[1]), normed.dtype)], axis=0)
    outgoing = jnp.take(padded, source_row, axis=0).reshape(expert_count, capacity, normed.shape[1])
    return (outgoing, slot_index)


def combine_rows(returned, slot_index, weight):
    flat_out = returned.reshape(-1, returned.shape[2])
    picked = jnp.take(flat_out, slot_index, axis=0).reshape(
        weight.shape[0], weight.shape[1], flat_out.shape[1]
    )
    return jnp.sum(weight[:, :, None] * picked.astype(jnp.float32), axis=1)


MESH = pl.DeviceIdType.MESH
group_size = 4


def flip(index, bit):
    return index + bit - 2 * bit * ((index // bit) % 2)


def experts_kernel(
    dims,
    normed,
    meta,
    gate_piece,
    up_piece,
    own_gate,
    own_up,
    own_down,
    gain,
    shift,
    out,
    gate_a,
    up_a,
    down_a,
    gate_b,
    up_b,
    down_b,
    rows_in,
    meta_in,
    picked,
    spread,
    slot_weight,
    hidden,
    weighted,
    partial,
    passing,
    arrived,
    load_sems,
    send_sems,
    recv_sems,
):
    slots, expert_count = dims
    rows, width = normed.shape
    half = rows // 2
    ff = own_gate.shape[2]
    piece = gate_piece.shape[1]
    sp, tp = lax.axis_index("sp"), lax.axis_index("tp")
    to_y = {"sp": flip(sp, 1)}
    to_z = {"sp": flip(sp, 2)}
    to_far = {"sp": flip(sp, group_size)}
    to_x = {"tp": flip(tp, 2)}
    to_core = {"tp": flip(tp, 1)}

    loads = [
        pltpu.make_async_copy(own_gate.at[0], gate_a, load_sems.at[0]),
        pltpu.make_async_copy(own_up.at[0], up_a, load_sems.at[1]),
        pltpu.make_async_copy(own_down.at[0], down_a, load_sems.at[2]),
    ]
    for load in loads:
        load.start()

    barrier = pltpu.get_barrier_semaphore()
    peers = (to_y, to_z, to_far, to_x, to_core)
    for peer in peers:
        pl.semaphore_signal(barrier, inc=1, device_id=peer, device_id_type=MESH)
    pl.semaphore_wait(barrier, len(peers))

    made = []

    def send(src, dst, peer):
        index = len(made)
        copy = pltpu.make_async_remote_copy(
            src_ref=src,
            dst_ref=dst,
            send_sem=send_sems.at[index],
            recv_sem=recv_sems.at[index],
            device_id=peer,
            device_id_type=MESH,
        )
        copy.start()
        made.append(copy)
        return copy

    first, second = pl.ds(0, half), pl.ds(half, half)

    def cols(position):
        return pl.ds(pl.multiple_of(position * piece, piece), piece)

    mine, across, other, corner = cols(tp), cols(flip(tp, 2)), cols(flip(tp, 1)), None

    meta_y = send(meta, meta_in.at[0], to_y)
    meta_z = send(meta, meta_in.at[1], to_z)
    rows_y1 = send(normed.at[first], rows_in.at[0, first], to_y)
    rows_z2 = send(normed.at[second], rows_in.at[1, second], to_z)
    down_far = send(own_down.at[0, mine], down_b.at[mine], to_far)
    gate_x = send(gate_piece, gate_b.at[:, mine], to_x)
    up_x = send(up_piece, up_b.at[:, mine], to_x)
    gate_c = send(gate_piece, gate_b.at[:, mine], to_core)
    up_c = send(up_piece, up_b.at[:, mine], to_core)
    keep = [
        pltpu.make_async_copy(gate_piece, gate_b.at[:, mine], load_sems.at[3]),
        pltpu.make_async_copy(up_piece, up_b.at[:, mine], load_sems.at[4]),
    ]
    for load in keep:
        load.start()
    rows_y2 = send(normed.at[second], rows_in.at[0, second], to_y)
    rows_z1 = send(normed.at[first], rows_in.at[1, first], to_z)

    slot_ids = lax.broadcasted_iota(jnp.int32, (slots, rows), 0).astype(jnp.float32)
    experts = (sp, flip(sp, group_size))

    def select(position, row_ref, meta_ref):
        parts = []
        for which in range(2):
            slot_row = meta_ref[pl.ds(experts[which], 1), :]
            weight_row = meta_ref[pl.ds(expert_count + experts[which], 1), :]
            match = jnp.where(slot_ids == slot_row, 1.0, 0.0)
            slot_weight[position, pl.ds(which * slots, slots), :] = jnp.sum(
                match * weight_row, axis=1, keepdims=True
            )
            parts.append(match)
        match = jnp.concatenate(parts, axis=0)
        spread[position] = jnp.transpose(match).astype(jnp.bfloat16)
        match = match.astype(jnp.bfloat16)

        @pl.loop(0, 4)
        def _(step):
            wide = width // 4
            block = pl.ds(pl.multiple_of(step * wide, wide), wide)
            picked[position, :, block] = jnp.dot(
                match, row_ref[:, block], preferred_element_type=jnp.float32
            ).astype(jnp.bfloat16)

    def ffn(position, which, gate, up, down):
        where = pl.ds(which * slots, slots)

        @pl.loop(0, 2)
        def _(step):
            wide = ff // 2
            block = pl.ds(pl.multiple_of(step * wide, wide), wide)
            values = picked[position, where, :]
            gate_out = jnp.dot(values, gate[:, block], preferred_element_type=jnp.float32)
            up_out = jnp.dot(values, up[:, block], preferred_element_type=jnp.float32)
            hidden[:, block] = (gate_out / (1.0 + jnp.exp(-gate_out)) * up_out).astype(
                jnp.bfloat16
            )

        @pl.loop(0, 4)
        def _(step):
            wide = width // 4
            block = pl.ds(pl.multiple_of(step * wide, wide), wide)
            result = jnp.dot(hidden[...], down[:, block], preferred_element_type=jnp.float32)
            weighted[position, where, block] = (
                result * slot_weight[position, where, :]
            ).astype(jnp.bfloat16)

    def gather_back(position):
        @pl.loop(0, 4)
        def _(step):
            wide = width // 4
            block = pl.ds(pl.multiple_of(step * wide, wide), wide)
            partial[position, :, block] = jnp.dot(
                spread[position], weighted[position, :, block], preferred_element_type=jnp.float32
            ).astype(jnp.bfloat16)

    own, from_y, from_z, from_corner = 3, 0, 1, 2
    select(own, normed, meta)
    for load in loads:
        load.wait()
    ffn(own, 0, gate_a, up_a, down_a)

    meta_y.wait_recv()
    meta_corner = send(meta_in.at[0], meta_in.at[2], to_z)
    rows_y1.wait_recv()
    rows_corner1 = send(rows_in.at[0, first], rows_in.at[2, first], to_z)
    rows_z2.wait_recv()
    rows_corner2 = send(rows_in.at[1, second], rows_in.at[2, second], to_y)
    gate_x.wait_recv()
    gate_relay = send(gate_b.at[:, across], gate_b.at[:, across], to_core)
    up_x.wait_recv()
    up_relay = send(up_b.at[:, across], up_b.at[:, across], to_core)
    down_far.wait_recv()
    down_x = send(down_b.at[mine], down_b.at[mine], to_x)
    down_c = send(down_b.at[mine], down_b.at[mine], to_core)

    rows_y2.wait_recv()
    select(from_y, rows_in.at[0], meta_in.at[0])
    ffn(from_y, 0, gate_a, up_a, down_a)
    meta_z.wait_recv()
    rows_z1.wait_recv()
    select(from_z, rows_in.at[1], meta_in.at[1])
    ffn(from_z, 0, gate_a, up_a, down_a)
    down_x.wait_recv()
    down_relay = send(down_b.at[across], down_b.at[across], to_core)
    meta_corner.wait_recv()
    rows_corner1.wait_recv()
    rows_corner2.wait_recv()
    select(from_corner, rows_in.at[2], meta_in.at[2])
    ffn(from_corner, 0, gate_a, up_a, down_a)
    for load in keep:
        load.wait()
    for copy in (gate_c, up_c, gate_relay, up_relay, down_c, down_relay):
        copy.wait_recv()

    ffn(from_corner, 1, gate_b, up_b, down_b)
    gather_back(from_corner)
    pass_y = send(partial.at[from_corner, first], passing.at[0], to_y)
    pass_z = send(partial.at[from_corner, second], passing.at[1], to_z)
    ffn(from_y, 1, gate_b, up_b, down_b)
    gather_back(from_y)
    back_y1 = send(partial.at[from_y, first], arrived.at[0, first], to_y)
    ffn(from_z, 1, gate_b, up_b, down_b)
    gather_back(from_z)
    back_z2 = send(partial.at[from_z, second], arrived.at[1, second], to_z)

    def add_passing(position, where, slot):
        partial[position, where, :] = (
            partial[position, where, :].astype(jnp.float32) + passing[slot].astype(jnp.float32)
        ).astype(jnp.bfloat16)

    pass_y.wait_recv()
    add_passing(from_z, first, 0)
    back_z1 = send(partial.at[from_z, first], arrived.at[1, first], to_z)
    pass_z.wait_recv()
    add_passing(from_y, second, 1)
    back_y2 = send(partial.at[from_y, second], arrived.at[0, second], to_y)
    ffn(own, 1, gate_b, up_b, down_b)
    for copy in (back_y1, back_z2, back_z1, back_y2):
        copy.wait_recv()

    @pl.loop(0, rows // 64)
    def _(step):
        block = pl.ds(pl.multiple_of(step * 64, 64), 64)
        routed = jnp.dot(spread[own, block, :], weighted[own], preferred_element_type=jnp.float32)
        routed = routed + arrived[0, block, :].astype(jnp.float32)
        routed = routed + arrived[1, block, :].astype(jnp.float32)
        values = skip_scale * normed[block, :].astype(jnp.float32) + routed
        out[block, :] = layer_norm(values, gain[...], shift[...]).astype(jnp.bfloat16)

    for copy in made:
        copy.wait_send()


def routing_table(chosen, weight, expert_count, capacity):
    rows = chosen.shape[0]
    half = rows // 2
    onehot = (
        chosen[:, :, None] == jnp.arange(expert_count, dtype=jnp.int32)[None, None, :]
    ).astype(jnp.float32)
    named = jnp.sum(onehot, axis=1)
    before = jnp.tril(jnp.ones((half, half), jnp.bfloat16), -1)
    rank = jnp.einsum(
        "ab,hbe->hae",
        before,
        named.reshape(2, half, expert_count).astype(jnp.bfloat16),
        preferred_element_type=jnp.float32,
    )
    rank = rank + jnp.arange(2, dtype=jnp.float32)[:, None, None] * capacity
    slot = jnp.where(named > 0, rank.reshape(rows, expert_count), -1.0)
    share = jnp.sum(onehot * weight[:, :, None], axis=1)
    return jnp.concatenate([slot, share], axis=1).T


def near_experts(
    normed, weight, routes, pieces, expert_gate, expert_up, expert_down, ffn_gain, ffn_shift
):
    expert_count = lax.axis_size("sp")
    rows, width = normed.shape
    ff = expert_gate.shape[2]
    capacity = rows // 2 * routes.shape[1] * 2 // expert_count
    slots = 2 * capacity
    meta = routing_table(routes, weight, expert_count, capacity)
    vmem = pl.BlockSpec(memory_space=pltpu.VMEM)
    anywhere = pl.BlockSpec(memory_space=pl.ANY)
    bf16 = jnp.bfloat16
    return pl.pallas_call(
        functools.partial(experts_kernel, (slots, expert_count)),
        out_shape=jax.ShapeDtypeStruct((rows, width), bf16),
        in_specs=[vmem, vmem] + [anywhere] * 5 + [vmem, vmem],
        out_specs=vmem,
        scratch_shapes=[
            pltpu.VMEM((width, ff), bf16),
            pltpu.VMEM((width, ff), bf16),
            pltpu.VMEM((ff, width), bf16),
            pltpu.VMEM((width, ff), bf16),
            pltpu.VMEM((width, ff), bf16),
            pltpu.VMEM((ff, width), bf16),
            pltpu.VMEM((3, rows, width), bf16),
            pltpu.VMEM((3,) + meta.shape, jnp.float32),
            pltpu.VMEM((4, 2 * slots, width), bf16),
            pltpu.VMEM((4, rows, 2 * slots), bf16),
            pltpu.VMEM((4, 2 * slots, 1), jnp.float32),
            pltpu.VMEM((slots, ff), bf16),
            pltpu.VMEM((4, 2 * slots, width), bf16),
            pltpu.VMEM((3, rows, width), bf16),
            pltpu.VMEM((2, rows // 2, width), bf16),
            pltpu.VMEM((2, rows, width), bf16),
            pltpu.SemaphoreType.DMA((5,)),
            pltpu.SemaphoreType.DMA((25,)),
            pltpu.SemaphoreType.DMA((25,)),
        ],
        compiler_params=pltpu.CompilerParams(
            collective_id=0, has_side_effects=True, vmem_limit_bytes=60 * 1024 * 1024
        ),
    )(
        normed,
        meta,
        pieces[0],
        pieces[1],
        expert_gate,
        expert_up,
        expert_down,
        ffn_gain[None, :],
        ffn_shift[None, :],
    )


def on_device(
    residual,
    pool_input,
    doc_ids,
    pool_map,
    pool_scale,
    out_weight,
    mix_gain,
    mix_shift,
    group_router,
    expert_router,
    expert_gate,
    expert_up,
    expert_down,
    routes,
    ffn_gain,
    ffn_shift,
):
    seq_rows = pool_input.shape[0]
    reach_rows = 15
    expert_count = lax.axis_size("sp")
    tp_count = lax.axis_size("tp")
    near = expert_count == 2 * group_size and tp_count == group_size
    if near:
        piece = expert_gate.shape[2] // tp_count
        begin = lax.axis_index("tp") * piece
        swap = [(i, (i + group_size) % expert_count) for i in range(expert_count)]
        pieces = [
            lax.ppermute(lax.dynamic_slice_in_dim(part[0], begin, piece, axis=1), "sp", swap)
            for part in (expert_gate, expert_up)
        ]
    window = jnp.left_shift(jnp.int32(2), lax.axis_index("tp"))
    first_row = lax.axis_index("sp") * seq_rows
    tail_values, tail_docs = from_behind(
        (pool_input[seq_rows - reach_rows :], doc_ids[seq_rows - reach_rows :]), "sp", 1
    )
    source = jnp.concatenate([tail_values, pool_input], axis=0).astype(jnp.float32)
    all_docs = jnp.concatenate([tail_docs, doc_ids], axis=0)
    positions = first_row - reach_rows + jnp.arange(seq_rows + reach_rows, dtype=jnp.int32)
    running = jnp.zeros((seq_rows, source.shape[1]), jnp.float32)
    weight_sum = jnp.zeros((seq_rows, 1), jnp.float32)
    for offset in range(reach_rows + 1):
        begin_row = reach_rows - offset
        earlier = source[begin_row : begin_row + seq_rows]
        keep_mask = (
            (all_docs[begin_row : begin_row + seq_rows] == doc_ids)
            & (positions[begin_row : begin_row + seq_rows] >= 0)
            & (offset < window)
        )
        same_doc = keep_mask.astype(jnp.float32)[:, None]
        running = running + same_doc * earlier
        weight_sum = weight_sum + same_doc
    pooled = (running / weight_sum - source[reach_rows:]).astype(jnp.bfloat16)
    mixed = (jnp.dot(pooled, pool_map[0], preferred_element_type=jnp.float32) * pool_scale).astype(
        jnp.bfloat16
    )
    row_count = seq_rows // tp_count
    blocks = mixed.reshape(tp_count, row_count, mixed.shape[1])
    branch = jnp.einsum(
        "abc,cd->abd",
        lax.all_to_all(blocks, "tp", split_axis=0, concat_axis=2, tiled=True),
        out_weight,
        preferred_element_type=jnp.float32,
    )[0]
    normed = layer_norm(
        skip_scale * residual.astype(jnp.float32) + branch, mix_gain, mix_shift
    ).astype(jnp.bfloat16)
    weight = route_weights(normed, routes, group_router, expert_router)
    if near:
        return near_experts(
            normed, weight, routes, pieces, expert_gate, expert_up, expert_down, ffn_gain, ffn_shift
        )
    half_most = row_count * routes.shape[1] // expert_count
    half_rows = row_count // 2
    routed_parts = []
    for piece_index in range(2):
        rows_here = slice(piece_index * half_rows, (piece_index + 1) * half_rows)
        outgoing, slot_index = fill_slots(
            normed[rows_here], routes[rows_here], half_most, expert_count
        )
        returned = lax.all_to_all(
            expert_ffn(
                lax.all_to_all(outgoing, "sp", split_axis=0, concat_axis=0, tiled=True),
                expert_gate,
                expert_up,
                expert_down,
            ),
            "sp",
            split_axis=0,
            concat_axis=0,
            tiled=True,
        )
        routed_parts.append(combine_rows(returned, slot_index, weight[rows_here]))
    routed = jnp.concatenate(routed_parts, axis=0)
    return layer_norm(skip_scale * normed.astype(jnp.float32) + routed, ffn_gain, ffn_shift).astype(
        jnp.bfloat16
    )


def solution(mesh):
    in_specs = (
        P(("sp", "tp"), None),
        P("sp", "tp"),
        P("sp"),
        P("tp", None, None),
        P("tp"),
        P(),
        P(),
        P(),
        P(),
        P(),
        P("sp", None, None),
        P("sp", None, None),
        P("sp", None, None),
        P(("sp", "tp"), None),
        P(),
        P(),
    )
    out_specs = P(("sp", "tp"), None)
    return jax.shard_map(
        on_device, mesh=mesh, in_specs=in_specs, out_specs=out_specs, check_vma=False
    )
```

profile of v0, /device:TPU:0, one launch (start us, length us, event | category | flops | bytes accessed | tf_op | source)
XLA Modules:
  0.0 155.0 jit_solution(14191232178174492312)
XLA Ops:
  0.0 0.0 copy-start
  0.0 0.0 copy-start.11
  0.0 0.0 copy-start.3
  0.0 0.0 copy-start.12
  0.0 0.8 slice.151
  0.8 4.9 %collective-permute-start.1 = (s32[15]{0:T(128)S(1)}, s32[15]{0:T(128)S(1)}, u32[]{:S(2)}, u32[]{:S(2)}) collective-permute-start(s32[15]{0:T(128)S(1)} %slice.151), channel_id=1, source_target_pairs={{0,4},{4,8},{8,12},{12,16},{16,20},{20,24},{24,28},{1,5},{5,9},{9,... | collective-permute-start | bytes 188 | tf_op jit(solution)/shard_map/ppermute | solution.py:17
  5.7 0.7 slice.149
  6.4 3.4 %collective-permute-start = (bf16[15,256]{1,0:T(8,128)(2,1)S(1)}, bf16[15,256]{1,0:T(8,128)(2,1)S(1)}, u32[]{:S(2)}, u32[]{:S(2)}) collective-permute-start(bf16[15,256]{1,0:T(8,128)(2,1)S(1)} %slice.149), channel_id=1, source_target_pairs={{0,4},{4,8},{8,12},{12,16},{16,20},{20,24},{24,28},{1,5},{5,9},{9,... | collective-permute-start | bytes 23048 | tf_op jit(solution)/shard_map/ppermute | solution.py:17
  9.9 1.1 dynamic-slice_bitcast_fusion.1
  11.0 2.7 %collective-permute-start.2 = (bf16[2048,128]{1,0:T(8,128)(2,1)S(1)}, bf16[2048,128]{1,0:T(8,128)(2,1)S(1)}, u32[]{:S(2)}, u32[]{:S(2)}) collective-permute-start(bf16[2048,128]{1,0:T(8,128)(2,1)S(1)} %dynamic-slice_bitcast_fusion.1), channel_id=1, source_target_pairs={{0,16},{4,20},{8,24},{12,28},{16,0},{20,4},{24,8},{28,12},{1,17},{... | collective-permute-start | bytes 1572872 | tf_op jit(solution)/shard_map/ppermute | solution.py:432
  13.6 1.9 %dynamic-slice_bitcast_fusion = bf16[2048,128]{1,0:T(8,128)(2,1)} fusion(bf16[1,2048,512]{2,1,0:T(8,128)(2,1)} %own_up.1, s32[]{:T(128)S(6)} %select_n.30), kind=kLoop, calls=%fused_computation.43 | loop fusion | bytes 1048580 | tf_op jit(solution)/shard_map/dynamic_slice | solution.py:432
  15.5 0.3 collective-permute-start.3
  15.8 0.0 collective-permute-done.1
  15.8 0.0 copy-done.11
  15.8 0.1 add_add_fusion
  16.0 0.0 collective-permute-done
  16.0 0.0 copy-done.3
  16.0 0.1 maximum_convert_fusion
  16.1 0.0 copy-done
  16.1 0.0 copy-done.12
  16.1 4.5 %fusion = bf16[1024,256]{1,0:T(8,128)(2,1)S(1)} fusion(f32[256]{0:T(256)S(1)} %copy-done.12, f32[1039,256]{1,0:T(8,128)S(1)} %maximum_convert_fusion, f32[1024]{0:T(1024)S(1)} %get-tuple-element.7, f32[1024]{0:T(1024)S(1)} %get-tuple-element.23, f32[1024]{0:T(1024)S(1)} %get-tuple-element.22, f32[1024]{0:T(1024)S(1)} %get-tuple-element.21, ...), kind=kOutput, calls=%fused_computation.4 | convolution fusion | flops 143654912 | bytes 17503232 | tf_op jit(solution)/shard_map/dot_general | solution.py:457
  20.6 0.0 copy-start.7
  20.6 0.0 copy-start.2
  20.6 1.0 copy.26
  21.6 3.5 %all-to-all-start = ((bf16[4,256,256]{1,2,0:T(8,128)(2,1)}), bf16[4,256,256]{1,2,0:T(8,128)(2,1)S(1)}, u32[]{:S(2)}, u32[]{:S(2)}) async-start(bf16[4,256,256]{1,2,0:T(8,128)(2,1)} %copy.26), calls=%async_computation | async-start | bytes 1048576 | tf_op jit(solution)/shard_map/all_to_all | solution.py:464
  25.1 0.0 copy-done.7
  25.2 8.7 %all-to-all-done = bf16[4,256,256]{1,2,0:T(8,128)(2,1)S(1)} async-done(((bf16[4,256,256]{1,2,0:T(8,128)(2,1)}), bf16[4,256,256]{1,2,0:T(8,128)(2,1)S(1)}, u32[]{:S(2)}, u32[]{:S(2)}) %all-to-all-start) | async-done | bytes 524320 | tf_op jit(solution)/shard_map/all_to_all | solution.py:464
  33.9 0.0 copy-done.2
  33.9 3.5 %fusion.122 = (f32[256]{0:T(256)S(1)}, f32[256,2048]{1,0:T(8,128)S(1)}) fusion(bf16[256,1024]{0,1:T(8,128)(2,1)S(1)} %bitcast.35, bf16[1024,2048]{1,0:T(8,128)(2,1)} %param.21, bf16[256,2048]{1,0:T(8,128)(2,1)S(1)} %copy-done.2), kind=kOutput, calls=%fused_computation.196 | convolution fusion | flops 1075838720 | bytes 7865344 | tf_op jit(solution)/shard_map/abc,cd->abd/dot_general | solution.py:462
  37.4 0.0 copy-start.9
  37.4 0.0 copy-start.10
  37.5 0.4 multiply_reduce_fusion
  37.8 0.0 copy-start.6
  37.8 0.3 copy-done.9
  38.1 0.0 copy-done.10
  38.2 0.0 copy-start.8
  38.2 0.5 add_convert_fusion.normed
  38.6 0.0 copy-done.6
  38.6 0.0 copy-start.1
  38.6 0.4 fusion.124
  39.1 0.0 copy-done.8
  39.1 0.4 fusion.123
  39.6 0.2 fusion.2
  39.8 0.6 maximum_bitcast_fusion.meta
  40.4 8.2 %collective-permute-done.2.gate_piece = bf16[2048,128]{1,0:T(8,128)(2,1)S(1)} collective-permute-done((bf16[2048,128]{1,0:T(8,128)(2,1)S(1)}, bf16[2048,128]{1,0:T(8,128)(2,1)S(1)}, u32[]{:S(2)}, u32[]{:S(2)}) %collective-permute-start.2) | collective-permute-done | bytes 524320 | tf_op jit(solution)/shard_map/ppermute | solution.py:432
  48.6 0.0 copy-start.4
  48.6 10.1 %collective-permute-done.3.up_piece = bf16[2048,128]{1,0:T(8,128)(2,1)S(1)} collective-permute-done((bf16[2048,128]{1,0:T(8,128)(2,1)}, bf16[2048,128]{1,0:T(8,128)(2,1)S(1)}, u32[]{:S(2)}, u32[]{:S(2)}) %collective-permute-start.3) | collective-permute-done | bytes 524320 | tf_op jit(solution)/shard_map/ppermute | solution.py:432
  58.7 0.0 copy-start.5
  58.7 0.0 copy-done.1
  58.7 0.0 copy-done.4
  58.7 0.8 copy-done.5
  59.5 93.1 %shard_map.154 = bf16[256,2048]{1,0:T(8,128)(2,1)} custom-call(bf16[256,2048]{1,0:T(8,128)(2,1)} %copy-done.1, f32[16,256]{1,0:T(8,128)} %maximum_bitcast_fusion.meta, bf16[2048,128]{1,0:T(8,128)(2,1)} %copy-done.4, bf16[2048,128]{1,0:T(8,128)(2,1)} %copy-done.5, bf16[1,2048,512]{2,1,0:T(8,128)(2,1)} %own_gate.1, bf16[1,2048,512]{2,1,0:T(8,128)(2,1)} %own_up.1, ...), custom_call_target="tpu_custom_call" | custom-call | tf_op jit(solution)/shard_map/pallas_call | solution.py:362
  152.7 2.3 %copy.28 = bf16[256,2048]{1,0:T(8,128)(2,1)} copy(bf16[256,2048]{1,0:T(8,128)(2,1)} %shard_map.154) | data formatting | bytes 2097152
  (12 shorter events, 0.1 us)
Async XLA Ops:
  0.0 16.1 %copy-start = (bf16[1,256,256]{2,1,0:T(8,128)(2,1)S(1)}, bf16[1,256,256]{2,1,0:T(8,128)(2,1)}, u32[]{:S(2)}) copy-start(bf16[1,256,256]{2,1,0:T(8,128)(2,1)} %param.19) | copy-start | bytes 393220
  0.0 15.8 %copy-start.11 = (s32[1024]{0:T(1024)S(1)}, s32[1024]{0:T(1024)}, u32[]{:S(2)}) copy-start(s32[1024]{0:T(1024)} %param.18) | copy-start | bytes 12292
  0.0 16.0 %copy-start.3 = (bf16[1024,256]{1,0:T(8,128)(2,1)S(1)}, bf16[1024,256]{1,0:T(8,128)(2,1)}, u32[]{:S(2)}) copy-start(bf16[1024,256]{1,0:T(8,128)(2,1)} %param.17) | copy-start | bytes 1572868
  0.0 16.1 %copy-start.12 = (f32[256]{0:T(256)S(1)}, f32[256]{0:T(256)}, u32[]{:S(2)}) copy-start(f32[256]{0:T(256)} %param.20) | copy-start | bytes 3076
  0.8 15.0 %collective-permute-start.1 = (s32[15]{0:T(128)S(1)}, s32[15]{0:T(128)S(1)}, u32[]{:S(2)}, u32[]{:S(2)}) collective-permute-start(s32[15]{0:T(128)S(1)} %slice.151), channel_id=1, source_target_pairs={{0,4},{4,8},{8,12},{12,16},{16,20},{20,24},{24,28},{1,5},{5,9},{9,... | collective-permute-start | bytes 188 | tf_op jit(solution)/shard_map/ppermute | solution.py:17
  6.4 9.5 %collective-permute-start = (bf16[15,256]{1,0:T(8,128)(2,1)S(1)}, bf16[15,256]{1,0:T(8,128)(2,1)S(1)}, u32[]{:S(2)}, u32[]{:S(2)}) collective-permute-start(bf16[15,256]{1,0:T(8,128)(2,1)S(1)} %slice.149), channel_id=1, source_target_pairs={{0,4},{4,8},{8,12},{12,16},{16,20},{20,24},{24,28},{1,5},{5,9},{9,... | collective-permute-start | bytes 23048 | tf_op jit(solution)/shard_map/ppermute | solution.py:17
  11.0 37.7 %collective-permute-start.2 = (bf16[2048,128]{1,0:T(8,128)(2,1)S(1)}, bf16[2048,128]{1,0:T(8,128)(2,1)S(1)}, u32[]{:S(2)}, u32[]{:S(2)}) collective-permute-start(bf16[2048,128]{1,0:T(8,128)(2,1)S(1)} %dynamic-slice_bitcast_fusion.1), channel_id=1, source_target_pairs={{0,16},{4,20},{8,24},{12,28},{16,0},{20,4},{24,8},{28,12},{1,17},{... | collective-permute-start | bytes 1572872 | tf_op jit(solution)/shard_map/ppermute | solution.py:432
  15.5 43.3 %collective-permute-start.3 = (bf16[2048,128]{1,0:T(8,128)(2,1)}, bf16[2048,128]{1,0:T(8,128)(2,1)S(1)}, u32[]{:S(2)}, u32[]{:S(2)}) collective-permute-start(bf16[2048,128]{1,0:T(8,128)(2,1)} %dynamic-slice_bitcast_fusion), channel_id=1, source_target_pairs={{0,16},{4,20},{8,24},{12,28},{16,0},{20,4},{24,8},{28,12},{1,17},{... | collective-permute-start | bytes 1572872 | tf_op jit(solution)/shard_map/ppermute | solution.py:432
  20.6 4.5 %copy-start.7 = (s32[256,2]{0,1:T(2,128)S(1)}, s32[256,2]{0,1:T(2,128)}, u32[]{:S(2)}) copy-start(s32[256,2]{0,1:T(2,128)} %param.29) | copy-start | bytes 6148
  20.6 13.3 %copy-start.2 = (bf16[256,2048]{1,0:T(8,128)(2,1)S(1)}, bf16[256,2048]{1,0:T(8,128)(2,1)}, u32[]{:S(2)}) copy-start(bf16[256,2048]{1,0:T(8,128)(2,1)} %param.16) | copy-start | bytes 3145732
  21.6 12.3 %all-to-all-start = ((bf16[4,256,256]{1,2,0:T(8,128)(2,1)}), bf16[4,256,256]{1,2,0:T(8,128)(2,1)S(1)}, u32[]{:S(2)}, u32[]{:S(2)}) async-start(bf16[4,256,256]{1,2,0:T(8,128)(2,1)} %copy.26), calls=%async_computation | async-start | bytes 1048576 | tf_op jit(solution)/shard_map/all_to_all | solution.py:464
  37.4 0.7 copy-start.9
  37.4 0.7 copy-start.10
  37.8 0.8 copy-start.6
  38.2 0.9 copy-start.8
  38.6 20.1 %copy-start.1 = (bf16[256,2048]{1,0:T(8,128)(2,1)}, bf16[256,2048]{1,0:T(8,128)(2,1)S(1)}, u32[]{:S(2)}) copy-start(bf16[256,2048]{1,0:T(8,128)(2,1)S(1)} %add_convert_fusion.normed) | copy-start | bytes 3145732
  48.6 10.1 %copy-start.4 = (bf16[2048,128]{1,0:T(8,128)(2,1)}, bf16[2048,128]{1,0:T(8,128)(2,1)S(1)}, u32[]{:S(2)}) copy-start(bf16[2048,128]{1,0:T(8,128)(2,1)S(1)} %collective-permute-done.2.gate_piece) | copy-start | bytes 1572868
  58.7 0.8 copy-start.5
where the time goes:
time: 156 us; the launch traced here: 155 us
  Pallas kernels  93.1 us (60%)
  waiting for transfers between devices  27.1 us (17%)
  starting transfers between devices  14.8 us (9%)
  matrix products  8.99 us (6%)
  local copies, waits for them, and re-layouts  8.95 us (6%)
  other arithmetic  1.81 us (1%)
    pallas_call x1, Pallas kernels, near_experts(): pl.pallas_call(functools.partial(experts_kernel, (slots, expert_count)),...  93.1 us
    ppermute x2, waiting for transfers between devices, on_device(): lax.ppermute(lax.dynamic_slice_in_dim(part[0], begin, piece, axis=1), 'sp...  18.3 us
    all_to_all x1, waiting for transfers between devices, on_device(): lax.all_to_all(blocks, 'tp', split_axis=0, concat_axis=2, tiled=True)  8.73 us
    ppermute x2, starting transfers between devices, from_behind(): return lax.ppermute(block, axis, route)  8.31 us
    dot_general x1, matrix products, on_device(): jnp.dot(pooled, pool_map[0], preferred_element_type=jnp.float32)  4.46 us
    dot_general x1, matrix products, on_device(): jnp.einsum('abc,cd->abd', lax.all_to_all(blocks, 'tp', split_axis=0, conc...  3.55 us
    unnamed x27, local copies, waits for them, and re-layouts  3.47 us
    all_to_all x1, starting transfers between devices, on_device(): lax.all_to_all(blocks, 'tp', split_axis=0, concat_axis=2, tiled=True)  3.47 us
  transfers between devices with their start and end apart: 5, of which 3 were waited for; matrix products, arithmetic and copies ran while one was open for 10% of the time, Pallas kernels for 0%

commit v1 on v0

v1 whole, which is shorter than its diff:
```python
import functools

import jax
import jax.numpy as jnp
from jax import lax
from jax.experimental import pallas as pl
from jax.experimental.pallas import tpu as pltpu
from jax.sharding import PartitionSpec as P

skip_scale = 2.0**0.5
epsilon = 1e-05


def from_behind(block, axis, distance):
    devices = range(lax.axis_size(axis))
    route = [(i - distance, i) for i in devices if i - distance in devices]
    return lax.ppermute(block, axis, route)


def layer_norm(values, norm_gain, norm_shift):
    center = values - jnp.mean(values, axis=-1, keepdims=True)
    spread = jnp.mean(center * center, axis=-1, keepdims=True)
    return center * lax.rsqrt(spread + epsilon) * norm_gain + norm_shift


def route_weights(normed, chosen, group_router, expert_router):
    group_logits = jnp.dot(normed, group_router, preferred_element_type=jnp.float32)
    expert_logits = jnp.dot(normed, expert_router, preferred_element_type=jnp.float32)
    group_count = group_logits.shape[1]
    expert_count = expert_logits.shape[1]
    group_exp = jnp.exp(group_logits)
    group_prob = group_exp / jnp.sum(group_exp, axis=1, keepdims=True)
    expert_ids = jnp.arange(expert_count, dtype=jnp.int32)
    picked = jnp.sum(
        jnp.where(chosen[:, :, None] == expert_ids[None, None, :], expert_logits[:, None, :], 0.0),
        axis=2,
    )
    picked_exp = jnp.exp(picked)
    pair_share = picked_exp / jnp.sum(picked_exp, axis=1, keepdims=True)
    group_of = chosen // (expert_count // group_count)
    group_ids = jnp.arange(group_count, dtype=jnp.int32)
    group_share = jnp.sum(
        jnp.where(group_of[:, :, None] == group_ids[None, None, :], group_prob[:, None, :], 0.0),
        axis=2,
    )
    return group_share * pair_share


def expert_ffn(arrived, expert_gate, expert_up, expert_down):
    sources, slot_count, width = arrived.shape
    gathered = arrived.reshape(sources * slot_count, width)
    gate_out = jnp.dot(gathered, expert_gate[0], preferred_element_type=jnp.float32)
    up_out = jnp.dot(gathered, expert_up[0], preferred_element_type=jnp.float32)
    hidden = (jax.nn.silu(gate_out) * up_out).astype(jnp.bfloat16)
    result = jnp.dot(hidden, expert_down[0], preferred_element_type=jnp.float32).astype(
        jnp.bfloat16
    )
    return result.reshape(sources, slot_count, width)


def fill_slots(normed, chosen, capacity, expert_count):
    flat_routes = chosen.reshape(-1)
    entry_count = flat_routes.shape[0]
    onehot = (flat_routes[:, None] == jnp.arange(expert_count, dtype=jnp.int32)[None, :]).astype(
        jnp.int32
    )
    slot_rank = jnp.sum((jnp.cumsum(onehot, axis=0) - onehot) * onehot, axis=1)
    slot_index = flat_routes * capacity + slot_rank
    token_ids = jnp.arange(entry_count, dtype=jnp.int32) // chosen.shape[1]
    source_row = (
        jnp.full((expert_count * capacity,), normed.shape[0], jnp.int32)
        .at[slot_index]
        .set(token_ids)
    )
    padded = jnp.concatenate([normed, jnp.zeros((1, normed.shape[1]), normed.dtype)], axis=0)
    outgoing = jnp.take(padded, source_row, axis=0).reshape(expert_count, capacity, normed.shape[1])
    return (outgoing, slot_index)


def combine_rows(returned, slot_index, weight):
    flat_out = returned.reshape(-1, returned.shape[2])
    picked = jnp.take(flat_out, slot_index, axis=0).reshape(
        weight.shape[0], weight.shape[1], flat_out.shape[1]
    )
    return jnp.sum(weight[:, :, None] * picked.astype(jnp.float32), axis=1)


MESH = pl.DeviceIdType.MESH
group_size = 4
block = 128


def flip(index, bit):
    return index + bit - 2 * bit * ((index // bit) % 2)


def layer_kernel(
    dims,
    residual_hbm,
    pool_hbm,
    docs_hbm,
    map_hbm,
    scale_hbm,
    weight_hbm,
    mix_gain_hbm,
    mix_shift_hbm,
    group_router_hbm,
    expert_router_hbm,
    routes_hbm,
    own_gate,
    own_up,
    own_down,
    gain_hbm,
    shift_hbm,
    out,
    residual,
    source,
    docs,
    pool_map,
    pool_scale,
    out_weight,
    mix_gain,
    mix_shift,
    group_router,
    expert_router,
    routes,
    gain,
    shift,
    mixed_out,
    mixed_in,
    values,
    normed,
    meta,
    gate_a,
    up_a,
    down_a,
    gate_b,
    up_b,
    down_b,
    rows_in,
    meta_in,
    picked,
    spread,
    slot_weight,
    hidden,
    weighted,
    partial,
    passing,
    arrived,
    load_sems,
    send_sems,
    recv_sems,
):
    slots, expert_count = dims
    rows, width = normed.shape
    half = rows // 2
    ff = own_gate.shape[2]
    seq_rows, group_width = pool_hbm.shape
    reach = 16
    sp, tp = lax.axis_index("sp"), lax.axis_index("tp")
    sp_count = expert_count
    to_y = {"sp": flip(sp, 1)}
    to_z = {"sp": flip(sp, 2)}
    to_far = {"sp": flip(sp, group_size)}
    to_next = {"sp": (sp + 1) % sp_count}
    to_last = {"sp": (sp + sp_count - 1) % sp_count}
    to_x = {"tp": flip(tp, 2)}
    to_core = {"tp": flip(tp, 1)}
    to_diag = {"tp": flip(flip(tp, 2), 1)}
    inner = ((sp // 2 + 1) // 2) % 2 == 1

    barrier = pltpu.get_barrier_semaphore()
    peers = (to_y, to_z, to_far, to_next, to_last, to_x, to_core, to_diag)
    for peer in peers:
        pl.semaphore_signal(barrier, inc=1, device_id=peer, device_id_type=MESH)

    loads = []

    def load(src, dst):
        copy = pltpu.make_async_copy(src, dst, load_sems.at[len(loads)])
        copy.start()
        loads.append(copy)
        return copy

    load_source = load(pool_hbm, source.at[pl.ds(block, seq_rows)])
    load_docs = load(docs_hbm, docs.at[pl.ds(8, 8)])
    load_map = load(map_hbm.at[0], pool_map)
    load_scale = load(scale_hbm, pool_scale)
    front = [
        load(residual_hbm, residual),
        load(weight_hbm, out_weight),
        load(mix_gain_hbm, mix_gain),
        load(mix_shift_hbm, mix_shift),
        load(group_router_hbm, group_router),
        load(expert_router_hbm, expert_router),
        load(routes_hbm, routes),
    ]
    experts_in = [
        load(own_gate.at[0], gate_a),
        load(own_up.at[0], up_a),
        load(own_down.at[0], down_a),
    ]
    ends = [load(gain_hbm, gain), load(shift_hbm, shift)]

    source[pl.ds(0, block - reach), :] = jnp.zeros((block - reach, group_width), jnp.bfloat16)
    pl.semaphore_wait(barrier, len(peers))

    made = []

    def send(src, dst, peer, when=None):
        index = len(made)
        copy = pltpu.make_async_remote_copy(
            src_ref=src,
            dst_ref=dst,
            send_sem=send_sems.at[index],
            recv_sem=recv_sems.at[index],
            device_id=peer,
            device_id_type=MESH,
        )
        made.append(copy)
        if when is None:
            copy.start()
        else:
            pl.when(when)(copy.start)
        return copy

    tail_rows = send(
        pool_hbm.at[pl.ds(seq_rows - reach, reach)], source.at[pl.ds(block - reach, reach)], to_next
    )
    tail_docs = send(docs_hbm, docs.at[pl.ds(0, 8)], to_next)

    piece = ff // 4
    k_half = width // 2

    def cols(position):
        return pl.ds(pl.multiple_of(position * piece, piece), piece)

    mine, across = cols(tp), cols(flip(tp, 2))
    chunks = []
    for own, kept in ((own_gate, gate_b), (own_up, up_b)):
        for part in range(2):
            where = pl.ds(part * k_half, k_half)
            chunks.append(
                (own.at[0, where, mine], kept.at[where, mine], kept.at[where, across])
            )
    for part in range(2):
        where = pl.ds(part * k_half, k_half)
        chunks.append(
            (own_down.at[0, mine, where], down_b.at[mine, where], down_b.at[across, where])
        )
    far = [
        send(own, kept, to_far, None if index == 0 else inner)
        for index, (own, kept, beside) in enumerate(chunks)
    ]

    window = 2 * (1 + tp % 2) * (1 + 3 * (tp // 2))
    row_ids = lax.broadcasted_iota(jnp.int32, (block, 2 * block), 0)
    col_ids = lax.broadcasted_iota(jnp.int32, (block, 2 * block), 1)
    behind = row_ids + block - col_ids
    in_window = (behind >= 0) & (behind < window)
    first, second = pl.ds(0, half), pl.ds(half, half)
    halves = (first, second)
    destinations = (
        (flip(tp, 2), to_x),
        (flip(flip(tp, 2), 1), to_diag),
        (flip(tp, 1), to_core),
        (tp, None),
    )
    channels = pl.ds(pl.multiple_of(tp * group_width, group_width), group_width)
    load_source.wait()
    load_docs.wait()
    load_map.wait()
    load_scale.wait()

    mixed_sent = {0: [], 1: []}

    def mix(which):
        for owner, peer in destinations:
            index = owner * 2 + which
            start = pl.multiple_of(index * block, block)
            here = docs[pl.ds(index + 8, 1), :].astype(jnp.float32)
            before = docs[pl.ds(index + 7, 1), :].astype(jnp.float32)
            across_docs = jnp.concatenate([before, here], axis=1)
            down_docs = jnp.transpose(jnp.broadcast_to(here, (block, block)))
            down_docs = jnp.concatenate([down_docs, down_docs], axis=1)
            known = col_ids + (sp * seq_rows + start) >= block
            keep = jnp.where(in_window & known & (across_docs == down_docs), 1.0, 0.0)
            total = jnp.dot(
                keep.astype(jnp.bfloat16),
                source[pl.ds(start, 2 * block), :],
                preferred_element_type=jnp.float32,
            )
            count = jnp.sum(keep, axis=1, keepdims=True)
            center = source[pl.ds(start + block, block), :].astype(jnp.float32)
            pooled = (total / count - center).astype(jnp.bfloat16)
            mixed = jnp.dot(pooled, pool_map[...], preferred_element_type=jnp.float32)
            mixed = (mixed * pool_scale[...]).astype(jnp.bfloat16)
            if peer is None:
                mixed_in[which, :, channels] = mixed
            else:
                place = len(mixed_sent[0]) + len(mixed_sent[1])
                mixed_out[place] = mixed
                mixed_sent[which].append(
                    send(mixed_out.at[place], mixed_in.at[which, :, channels], peer)
                )

    mix(1)
    tail_rows.wait_recv()
    tail_docs.wait_recv()
    mix(0)

    slot_cols = lax.broadcasted_iota(jnp.int32, (half, half), 1)
    slot_rows = lax.broadcasted_iota(jnp.int32, (half, half), 0)
    earlier = jnp.where(slot_rows < slot_cols, 1.0, 0.0).astype(jnp.bfloat16)
    expert_ids = lax.broadcasted_iota(jnp.int32, (expert_count, half), 0)
    group_count = group_router.shape[0]
    transposed = (((1,), (1,)), ((), ()))

    def project(which):
        where = halves[which]
        for copy in mixed_sent[which]:
            copy.wait_recv()

        @pl.loop(0, 4)
        def _(step):
            wide = width // 4
            part = pl.ds(pl.multiple_of(step * wide, wide), wide)
            values[:, part] = skip_scale * residual[where, part].astype(jnp.float32) + jnp.dot(
                mixed_in[which], out_weight[:, part], preferred_element_type=jnp.float32
            )

        @pl.loop(0, half // 32)
        def _(step):
            part = pl.ds(pl.multiple_of(step * 32, 32), 32)
            normed[pl.ds(pl.multiple_of(which * half + step * 32, 32), 32), :] = layer_norm(
                values[part, :], mix_gain[...], mix_shift[...]
            ).astype(jnp.bfloat16)

    def route(which):
        where = halves[which]
        lines = normed[where, :]
        group_logits = lax.dot_general(
            group_router[...], lines, transposed, preferred_element_type=jnp.float32
        )
        expert_logits = lax.dot_general(
            expert_router[...], lines, transposed, preferred_element_type=jnp.float32
        )
        group_exp = jnp.exp(group_logits)
        group_prob = group_exp / jnp.sum(group_exp, axis=0, keepdims=True)
        named = (routes[0:1, where] == expert_ids) | (routes[1:2, where] == expert_ids)
        group_share = jnp.zeros((expert_count, half), jnp.float32)
        for group in range(group_count):
            group_share = jnp.where(
                expert_ids // (expert_count // group_count) == group,
                group_prob[group : group + 1, :],
                group_share,
            )
        picked_exp = jnp.where(named, jnp.exp(jnp.where(named, expert_logits, 0.0)), 0.0)
        share = group_share * (picked_exp / jnp.sum(picked_exp, axis=0, keepdims=True))
        ones = jnp.where(named, 1.0, 0.0)
        rank = jnp.dot(ones.astype(jnp.bfloat16), earlier, preferred_element_type=jnp.float32)
        meta[which, pl.ds(0, expert_count), :] = jnp.where(named, rank, -1.0)
        meta[which, pl.ds(expert_count, expert_count), :] = share

    for copy in front:
        copy.wait()
    rows_y, rows_z, meta_y, meta_z = {}, {}, {}, {}
    for which in (1, 0):
        where = halves[which]
        project(which)
        rows_y[which] = send(normed.at[where], rows_in.at[0, where], to_y)
        rows_z[which] = send(normed.at[where], rows_in.at[1, where], to_z)
        route(which)
        meta_y[which] = send(meta.at[which], meta_in.at[0, which], to_y)
        meta_z[which] = send(meta.at[which], meta_in.at[1, which], to_z)

    slot_ids = lax.broadcasted_iota(jnp.int32, (slots, half), 0).astype(jnp.float32)
    experts = (sp, flip(sp, group_size))

    def select(position, which, row_ref, meta_ref):
        parts = []
        for kind in range(2):
            slot_row = meta_ref[which, pl.ds(experts[kind], 1), :]
            weight_row = meta_ref[which, pl.ds(expert_count + experts[kind], 1), :]
            match = jnp.where(slot_ids == slot_row, 1.0, 0.0)
            slot_weight[kind, position, pl.ds(which * slots, slots), :] = jnp.sum(
                match * weight_row, axis=1, keepdims=True
            )
            parts.append(match)
        match = jnp.concatenate(parts, axis=0)
        spread[position, which] = jnp.transpose(match).astype(jnp.bfloat16)
        match = match.astype(jnp.bfloat16)

        @pl.loop(0, 4)
        def _(step):
            wide = width // 4
            part = pl.ds(pl.multiple_of(step * wide, wide), wide)
            found = jnp.dot(
                match, row_ref[halves[which], part], preferred_element_type=jnp.float32
            ).astype(jnp.bfloat16)
            for kind in range(2):
                picked[kind, position, pl.ds(which * slots, slots), part] = found[
                    kind * slots : (kind + 1) * slots
                ]

    def ffn(position, kind, gate, up, down):
        @pl.loop(0, 2)
        def _(step):
            wide = ff // 2
            part = pl.ds(pl.multiple_of(step * wide, wide), wide)
            lines = picked[kind, position]
            gate_out = jnp.dot(lines, gate[:, part], preferred_element_type=jnp.float32)
            up_out = jnp.dot(lines, up[:, part], preferred_element_type=jnp.float32)
            hidden[:, part] = (gate_out / (1.0 + jnp.exp(-gate_out)) * up_out).astype(jnp.bfloat16)

        @pl.loop(0, 4)
        def _(step):
            wide = width // 4
            part = pl.ds(pl.multiple_of(step * wide, wide), wide)
            result = jnp.dot(hidden[...], down[:, part], preferred_element_type=jnp.float32)
            result = (result * slot_weight[kind, position]).astype(jnp.bfloat16)
            for which in range(2):
                weighted[position, which, pl.ds(kind * slots, slots), part] = result[
                    which * slots : (which + 1) * slots
                ]

    def gather_back(position):
        for which in range(2):

            @pl.loop(0, 4)
            def _(step):
                wide = width // 4
                part = pl.ds(pl.multiple_of(step * wide, wide), wide)
                partial[position, halves[which], part] = jnp.dot(
                    spread[position, which],
                    weighted[position, which, :, part],
                    preferred_element_type=jnp.float32,
                ).astype(jnp.bfloat16)

    by_x, by_core, by_relay = [], [], []

    def pass_far(index):
        own, kept, beside = chunks[index]
        far[index].wait_recv()
        by_x.append(send(kept, kept, to_x))
        by_core.append(send(kept, kept, to_core))

    def pass_x(index):
        own, kept, beside = chunks[index]
        by_x[index].wait_recv()
        by_relay.append(send(beside, beside, to_core))

    own, from_y, from_z, from_corner = 3, 0, 1, 2
    select(own, 1, normed, meta)
    select(own, 0, normed, meta)
    for copy in experts_in:
        copy.wait()
    ffn(own, 0, gate_a, up_a, down_a)
    pass_far(0)

    rows_y[1].wait_recv()
    meta_y[1].wait_recv()
    corner_1 = send(rows_in.at[0, second], rows_in.at[2, second], to_z)
    corner_meta_1 = send(meta_in.at[0, 1], meta_in.at[2, 1], to_z)
    for index in range(1, len(chunks)):
        pl.when(jnp.logical_not(inner))(far[index].start)
    select(from_y, 1, rows_in.at[0], meta_in.at[0])
    rows_z[1].wait_recv()
    meta_z[1].wait_recv()
    select(from_z, 1, rows_in.at[1], meta_in.at[1])
    pass_x(0)
    rows_z[0].wait_recv()
    meta_z[0].wait_recv()
    corner_0 = send(rows_in.at[1, first], rows_in.at[2, first], to_y)
    corner_meta_0 = send(meta_in.at[1, 0], meta_in.at[2, 0], to_y)
    select(from_z, 0, rows_in.at[1], meta_in.at[1])
    ffn(from_z, 0, gate_a, up_a, down_a)
    rows_y[0].wait_recv()
    meta_y[0].wait_recv()
    select(from_y, 0, rows_in.at[0], meta_in.at[0])
    ffn(from_y, 0, gate_a, up_a, down_a)
    corner_1.wait_recv()
    corner_meta_1.wait_recv()
    select(from_corner, 1, rows_in.at[2], meta_in.at[2])
    corner_0.wait_recv()
    corner_meta_0.wait_recv()
    select(from_corner, 0, rows_in.at[2], meta_in.at[2])
    ffn(from_corner, 0, gate_a, up_a, down_a)
    for index in range(1, len(chunks)):
        pass_far(index)
        if index > 1:
            pass_x(index - 1)
    pass_x(len(chunks) - 1)
    for copy in by_core + by_relay:
        copy.wait_recv()

    ffn(from_corner, 1, gate_b, up_b, down_b)
    gather_back(from_corner)
    pass_y = send(partial.at[from_corner, first], passing.at[0], to_y)
    pass_z = send(partial.at[from_corner, second], passing.at[1], to_z)
    ffn(from_y, 1, gate_b, up_b, down_b)
    gather_back(from_y)
    back_y1 = send(partial.at[from_y, first], arrived.at[0, first], to_y)
    ffn(from_z, 1, gate_b, up_b, down_b)
    gather_back(from_z)
    back_z2 = send(partial.at[from_z, second], arrived.at[1, second], to_z)

    def add_passing(position, where, slot):
        partial[position, where, :] = (
            partial[position, where, :].astype(jnp.float32) + passing[slot].astype(jnp.float32)
        ).astype(jnp.bfloat16)

    ffn(own, 1, gate_b, up_b, down_b)
    pass_y.wait_recv()
    add_passing(from_z, first, 0)
    back_z1 = send(partial.at[from_z, first], arrived.at[1, first], to_z)
    pass_z.wait_recv()
    add_passing(from_y, second, 1)
    back_y2 = send(partial.at[from_y, second], arrived.at[0, second], to_y)
    for copy in ends:
        copy.wait()
    for copy in (back_y1, back_z2, back_z1, back_y2):
        copy.wait_recv()

    for which in range(2):

        @pl.loop(0, half // 64)
        def _(step):
            inside = pl.ds(pl.multiple_of(step * 64, 64), 64)
            part = pl.ds(pl.multiple_of(which * half + step * 64, 64), 64)
            routed = jnp.dot(
                spread[own, which, inside, :],
                weighted[own, which],
                preferred_element_type=jnp.float32,
            )
            routed = routed + arrived[0, part, :].astype(jnp.float32)
            routed = routed + arrived[1, part, :].astype(jnp.float32)
            total = skip_scale * normed[part, :].astype(jnp.float32) + routed
            out[part, :] = layer_norm(total, gain[...], shift[...]).astype(jnp.bfloat16)

    for copy in made:
        copy.wait_send()


def near_layer(
    residual,
    pool_input,
    doc_ids,
    pool_map,
    pool_scale,
    out_weight,
    mix_gain,
    mix_shift,
    group_router,
    expert_router,
    expert_gate,
    expert_up,
    expert_down,
    routes,
    ffn_gain,
    ffn_shift,
):
    expert_count = lax.axis_size("sp")
    rows, width = residual.shape
    ff = expert_gate.shape[2]
    seq_rows, group_width = pool_input.shape
    pool_width = out_weight.shape[0]
    group_count = group_router.shape[1]
    half = rows // 2
    slots = half * routes.shape[1] * 2 // expert_count
    anywhere = pl.BlockSpec(memory_space=pl.ANY)
    bf16, f32 = jnp.bfloat16, jnp.float32
    operands = (
        residual,
        pool_input,
        doc_ids.reshape(seq_rows // block, block),
        pool_map,
        pool_scale[None, :],
        out_weight,
        mix_gain[None, :],
        mix_shift[None, :],
        group_router.T,
        expert_router.T,
        routes.T,
        expert_gate,
        expert_up,
        expert_down,
        ffn_gain[None, :],
        ffn_shift[None, :],
    )
    return pl.pallas_call(
        functools.partial(layer_kernel, (slots, expert_count)),
        out_shape=jax.ShapeDtypeStruct((rows, width), bf16),
        in_specs=[anywhere] * len(operands),
        out_specs=pl.BlockSpec(memory_space=pltpu.VMEM),
        scratch_shapes=[
            pltpu.VMEM((rows, width), bf16),
            pltpu.VMEM((seq_rows + block, group_width), bf16),
            pltpu.VMEM((16, block), jnp.int32),
            pltpu.VMEM((group_width, group_width), bf16),
            pltpu.VMEM((1, group_width), f32),
            pltpu.VMEM((pool_width, width), bf16),
            pltpu.VMEM((1, width), f32),
            pltpu.VMEM((1, width), f32),
            pltpu.VMEM((group_count, width), bf16),
            pltpu.VMEM((expert_count, width), bf16),
            pltpu.VMEM(routes.shape[::-1], jnp.int32),
            pltpu.VMEM((1, width), f32),
            pltpu.VMEM((1, width), f32),
            pltpu.VMEM((6, block, group_width), bf16),
            pltpu.VMEM((2, half, pool_width), bf16),
            pltpu.VMEM((half, width), f32),
            pltpu.VMEM((rows, width), bf16),
            pltpu.VMEM((2, 2 * expert_count, half), f32),
            pltpu.VMEM((width, ff), bf16),
            pltpu.VMEM((width, ff), bf16),
            pltpu.VMEM((ff, width), bf16),
            pltpu.VMEM((width, ff), bf16),
            pltpu.VMEM((width, ff), bf16),
            pltpu.VMEM((ff, width), bf16),
            pltpu.VMEM((3, rows, width), bf16),
            pltpu.VMEM((3, 2, 2 * expert_count, half), f32),
            pltpu.VMEM((2, 4, 2 * slots, width), bf16),
            pltpu.VMEM((4, 2, half, 2 * slots), bf16),
            pltpu.VMEM((2, 4, 2 * slots, 1), f32),
            pltpu.VMEM((2 * slots, ff), bf16),
            pltpu.VMEM((4, 2, 2 * slots, width), bf16),
            pltpu.VMEM((3, rows, width), bf16),
            pltpu.VMEM((2, half, width), bf16),
            pltpu.VMEM((2, rows, width), bf16),
            pltpu.SemaphoreType.DMA((16,)),
            pltpu.SemaphoreType.DMA((64,)),
            pltpu.SemaphoreType.DMA((64,)),
        ],
        compiler_params=pltpu.CompilerParams(
            collective_id=0, has_side_effects=True, vmem_limit_bytes=60 * 1024 * 1024
        ),
    )(*operands)


def on_device(
    residual,
    pool_input,
    doc_ids,
    pool_map,
    pool_scale,
    out_weight,
    mix_gain,
    mix_shift,
    group_router,
    expert_router,
    expert_gate,
    expert_up,
    expert_down,
    routes,
    ffn_gain,
    ffn_shift,
):
    seq_rows = pool_input.shape[0]
    reach_rows = 15
    expert_count = lax.axis_size("sp")
    tp_count = lax.axis_size("tp")
    near = expert_count == 2 * group_size and tp_count == group_size
    near = near and residual.shape[0] == 2 * block and seq_rows == tp_count * residual.shape[0]
    if near:
        return near_layer(
            residual,
            pool_input,
            doc_ids,
            pool_map,
            pool_scale,
            out_weight,
            mix_gain,
            mix_shift,
            group_router,
            expert_router,
            expert_gate,
            expert_up,
            expert_down,
            routes,
            ffn_gain,
            ffn_shift,
        )
    window = jnp.left_shift(jnp.int32(2), lax.axis_index("tp"))
    first_row = lax.axis_index("sp") * seq_rows
    tail_values, tail_docs = from_behind(
        (pool_input[seq_rows - reach_rows :], doc_ids[seq_rows - reach_rows :]), "sp", 1
    )
    source = jnp.concatenate([tail_values, pool_input], axis=0).astype(jnp.float32)
    all_docs = jnp.concatenate([tail_docs, doc_ids], axis=0)
    positions = first_row - reach_rows + jnp.arange(seq_rows + reach_rows, dtype=jnp.int32)
    running = jnp.zeros((seq_rows, source.shape[1]), jnp.float32)
    weight_sum = jnp.zeros((seq_rows, 1), jnp.float32)
    for offset in range(reach_rows + 1):
        begin_row = reach_rows - offset
        earlier = source[begin_row : begin_row + seq_rows]
        keep_mask = (
            (all_docs[begin_row : begin_row + seq_rows] == doc_ids)
            & (positions[begin_row : begin_row + seq_rows] >= 0)
            & (offset < window)
        )
        same_doc = keep_mask.astype(jnp.float32)[:, None]
        running = running + same_doc * earlier
        weight_sum = weight_sum + same_doc
    pooled = (running / weight_sum - source[reach_rows:]).astype(jnp.bfloat16)
    mixed = (jnp.dot(pooled, pool_map[0], preferred_element_type=jnp.float32) * pool_scale).astype(
        jnp.bfloat16
    )
    row_count = seq_rows // tp_count
    blocks = mixed.reshape(tp_count, row_count, mixed.shape[1])
    branch = jnp.einsum(
        "abc,cd->abd",
        lax.all_to_all(blocks, "tp", split_axis=0, concat_axis=2, tiled=True),
        out_weight,
        preferred_element_type=jnp.float32,
    )[0]
    normed = layer_norm(
        skip_scale * residual.astype(jnp.float32) + branch, mix_gain, mix_shift
    ).astype(jnp.bfloat16)
    weight = route_weights(normed, routes, group_router, expert_router)
    half_most = row_count * routes.shape[1] // expert_count
    half_rows = row_count // 2
    routed_parts = []
    for piece_index in range(2):
        rows_here = slice(piece_index * half_rows, (piece_index + 1) * half_rows)
        outgoing, slot_index = fill_slots(
            normed[rows_here], routes[rows_here], half_most, expert_count
        )
        returned = lax.all_to_all(
            expert_ffn(
                lax.all_to_all(outgoing, "sp", split_axis=0, concat_axis=0, tiled=True),
                expert_gate,
                expert_up,
                expert_down,
            ),
            "sp",
            split_axis=0,
            concat_axis=0,
            tiled=True,
        )
        routed_parts.append(combine_rows(returned, slot_index, weight[rows_here]))
    routed = jnp.concatenate(routed_parts, axis=0)
    return layer_norm(skip_scale * normed.astype(jnp.float32) + routed, ffn_gain, ffn_shift).astype(
        jnp.bfloat16
    )


def solution(mesh):
    in_specs = (
        P(("sp", "tp"), None),
        P("sp", "tp"),
        P("sp"),
        P("tp", None, None),
        P("tp"),
        P(),
        P(),
        P(),
        P(),
        P(),
        P("sp", None, None),
        P("sp", None, None),
        P("sp", None, None),
        P(("sp", "tp"), None),
        P(),
        P(),
    )
    out_specs = P(("sp", "tp"), None)
    return jax.shard_map(
        on_device, mesh=mesh, in_specs=in_specs, out_specs=out_specs, check_vma=False
    )
```

time: 156 us -> 161 us (1.032)
  Pallas kernels: 93.1 us -> 158 us
  waiting for transfers between devices: 27.1 us -> 0 us
  starting transfers between devices: 14.8 us -> 0 us
  matrix products: 8.99 us -> 0 us
  local copies, waits for them, and re-layouts: 8.95 us -> 2.3 us
  other arithmetic: 1.81 us -> 0 us
    pallas_call x1, Pallas kernels: 93.1 us -> 158 us  [near_layer(): pl.pallas_call(functools.partial(layer_kernel, (slots, expert_count)), ou...]
    ppermute x4 -> x0, waiting for transfers between devices: 18.3 us -> none  [the longest x2 18.3 us: on_device(): lax.ppermute(lax.dynamic_slice_in_dim(part[0], begin, piece, axis=1), 'sp...]
    ppermute x4 -> x0, starting transfers between devices: 11.3 us -> none  [the longest x2 8.31 us: from_behind(): return lax.ppermute(block, axis, route)]
    dot_general x5 -> x0, matrix products: 8.99 us -> none  [the longest x1 4.46 us: on_device(): jnp.dot(pooled, pool_map[0], preferred_element_type=jnp.float32)]
    all_to_all x1 -> x0, waiting for transfers between devices: 8.73 us -> none  [on_device(): lax.all_to_all(blocks, 'tp', split_axis=0, concat_axis=2, tiled=True)]
    all_to_all x1 -> x0, starting transfers between devices: 3.47 us -> none  [on_device(): lax.all_to_all(blocks, 'tp', split_axis=0, concat_axis=2, tiled=True)]
    dynamic_slice x2 -> x0, local copies, waits for them, and re-layouts: 2.94 us -> none  [on_device(): lax.dynamic_slice_in_dim(part[0], begin, piece, axis=1)]
    unnamed x27 -> x1, local copies, waits for them, and re-layouts: 3.47 us -> 2.3 us
  transfers between devices with their start and end apart: 5 -> 0, of which waited for: 3 -> 0; matrix products, arithmetic and copies ran while one was open for 10% -> 0% of each run, Pallas kernels for 0% -> 0%
where the time goes in v1:
time: 161 us
  Pallas kernels  158 us (98%)
  local copies, waits for them, and re-layouts  2.3 us (1%)
    pallas_call x1, Pallas kernels, near_layer(): pl.pallas_call(functools.partial(layer_kernel, (slots, expert_count)), ou...  158 us

profile of v1, /device:TPU:0, one launch (start us, length us, event | category | flops | bytes accessed | tf_op | source)
XLA Modules:
  0.0 160.7 jit_solution(5290986145416127372)
XLA Ops:
  0.0 158.4 %shard_map.154 = bf16[256,2048]{1,0:T(8,128)(2,1)} custom-call(bf16[256,2048]{1,0:T(8,128)(2,1)} %residual_hbm.1, bf16[1024,256]{1,0:T(8,128)(2,1)} %pool_hbm.1, s32[8,128]{1,0:T(8,128)} %bitcast.15, bf16[1,256,256]{2,1,0:T(8,128)(2,1)} %map_hbm.1, f32[1,256]{1,0:T(1,128)} %bitcast.17, bf16[1024,2048]{1,0:T(8,128)(2,1)} %weight_hbm.1, f32[1,2048]{1,0:T(1,128)} %bitcast.11, ...), custom_call_target="tpu_custom_call" | custom-call | tf_op jit(solution)/shard_map/pallas_call | solution.py:591
  158.4 2.3 %copy.18 = bf16[256,2048]{1,0:T(8,128)(2,1)} copy(bf16[256,2048]{1,0:T(8,128)(2,1)} %shard_map.154) | data formatting | bytes 2097152

commit v2 on v1

--- a/solution.py
+++ b/solution.py
@@ -92,6 +92,10 @@
 
 def flip(index, bit):
     return index + bit - 2 * bit * ((index // bit) % 2)
+
+
+def opposite(index):
+    return flip(flip(index, 2), group_size)
 
 
 def layer_kernel(
@@ -147,6 +151,13 @@
     partial,
     passing,
     arrived,
+    hidden_out,
+    hidden_in,
+    late_a,
+    late_b,
+    late_spread,
+    late_weight,
+    late_rows,
     load_sems,
     send_sems,
     recv_sems,
@@ -157,20 +168,22 @@
     ff = own_gate.shape[2]
     seq_rows, group_width = pool_hbm.shape
     reach = 16
+    back_y = rows // 2
     sp, tp = lax.axis_index("sp"), lax.axis_index("tp")
     sp_count = expert_count
     to_y = {"sp": flip(sp, 1)}
     to_z = {"sp": flip(sp, 2)}
-    to_far = {"sp": flip(sp, group_size)}
+    to_far = {"sp": opposite(sp)}
     to_next = {"sp": (sp + 1) % sp_count}
     to_last = {"sp": (sp + sp_count - 1) % sp_count}
     to_x = {"tp": flip(tp, 2)}
     to_core = {"tp": flip(tp, 1)}
+    to_corner = {"sp": flip(flip(sp, 1), 2)}
     to_diag = {"tp": flip(flip(tp, 2), 1)}
     inner = ((sp // 2 + 1) // 2) % 2 == 1
 
     barrier = pltpu.get_barrier_semaphore()
-    peers = (to_y, to_z, to_far, to_next, to_last, to_x, to_core, to_diag)
+    peers = (to_y, to_z, to_corner, to_far, to_next, to_last, to_x, to_core, to_diag)
     for peer in peers:
         pl.semaphore_signal(barrier, inc=1, device_id=peer, device_id_type=MESH)
 
@@ -207,7 +220,7 @@
 
     made = []
 
-    def send(src, dst, peer, when=None):
+    def send(src, dst, peer, when=None, start=True):
         index = len(made)
         copy = pltpu.make_async_remote_copy(
             src_ref=src,
@@ -217,10 +230,10 @@
             device_id=peer,
             device_id_type=MESH,
         )
-        made.append(copy)
-        if when is None:
+        made.append((copy, when))
+        if start and when is None:
             copy.start()
-        else:
+        elif start:
             pl.when(when)(copy.start)
         return copy
 
@@ -229,29 +242,49 @@
     )
     tail_docs = send(docs_hbm, docs.at[pl.ds(0, 8)], to_next)
 
-    piece = ff // 4
-    k_half = width // 2
-
-    def cols(position):
-        return pl.ds(pl.multiple_of(position * piece, piece), piece)
-
-    mine, across = cols(tp), cols(flip(tp, 2))
-    chunks = []
-    for own, kept in ((own_gate, gate_b), (own_up, up_b)):
-        for part in range(2):
-            where = pl.ds(part * k_half, k_half)
-            chunks.append(
-                (own.at[0, where, mine], kept.at[where, mine], kept.at[where, across])
-            )
-    for part in range(2):
-        where = pl.ds(part * k_half, k_half)
-        chunks.append(
-            (own_down.at[0, mine, where], down_b.at[mine, where], down_b.at[across, where])
-        )
+    quarter = width // 4
+    late = ff // 2
+
+    def share(position):
+        return pl.ds(pl.multiple_of(position * quarter, quarter), quarter)
+
+    mine, across = share(tp), share(flip(tp, 2))
+    soon, later = pl.ds(0, late), pl.ds(late, late)
+    outer = jnp.logical_not(inner)
+    chunks = [
+        (own_gate.at[0, mine, soon], gate_b.at[mine, soon], gate_b.at[across, soon], None),
+        (own_up.at[0, mine, soon], up_b.at[mine, soon], up_b.at[across, soon], None),
+        (own_down.at[0, soon, mine], down_b.at[soon, mine], down_b.at[soon, across], None),
+        (own_gate.at[0, mine, later], gate_b.at[mine, later], gate_b.at[across, later], None),
+        (own_up.at[0, mine, later], up_b.at[mine, later], up_b.at[across, later], None),
+        (own_down.at[0, later, mine], down_b.at[later, mine], down_b.at[later, across], inner),
+        (own_down.at[0, later, mine], late_a.at[:, mine], late_a.at[:, across], outer),
+    ]
     far = [
-        send(own, kept, to_far, None if index == 0 else inner)
-        for index, (own, kept, beside) in enumerate(chunks)
+        send(own_part, kept, to_far, when, start=False)
+        for own_part, kept, beside, when in chunks
     ]
+    by_x = [
+        send(kept, kept, to_x, inner if when is inner else None, start=False)
+        for own_part, kept, beside, when in chunks
+    ]
+    by_core = [
+        send(kept, kept, to_core, inner if when is inner else None, start=False)
+        for own_part, kept, beside, when in chunks
+    ]
+    by_relay = [
+        send(beside, beside, to_core, inner if when is inner else None, start=False)
+        for own_part, kept, beside, when in chunks
+    ]
+
+    def start_far(indices, when):
+        @pl.when(when)
+        def _():
+            for index in indices:
+                far[index].start()
+
+    start_far((0, 1, 2), outer)
+    start_far((0, 1, 2, 3, 4, 5), inner)
 
     window = 2 * (1 + tp % 2) * (1 + 3 * (tp // 2))
     row_ids = lax.broadcasted_iota(jnp.int32, (block, 2 * block), 0)
@@ -321,20 +354,20 @@
         for copy in mixed_sent[which]:
             copy.wait_recv()
 
-        @pl.loop(0, 4)
+        @pl.loop(0, 4, unroll=2)
         def _(step):
             wide = width // 4
             part = pl.ds(pl.multiple_of(step * wide, wide), wide)
-            values[:, part] = skip_scale * residual[where, part].astype(jnp.float32) + jnp.dot(
+            values[where, part] = skip_scale * residual[where, part].astype(jnp.float32) + jnp.dot(
                 mixed_in[which], out_weight[:, part], preferred_element_type=jnp.float32
             )
 
-        @pl.loop(0, half // 32)
+        @pl.loop(0, half // 16, unroll=2)
         def _(step):
-            part = pl.ds(pl.multiple_of(step * 32, 32), 32)
-            normed[pl.ds(pl.multiple_of(which * half + step * 32, 32), 32), :] = layer_norm(
-                values[part, :], mix_gain[...], mix_shift[...]
-            ).astype(jnp.bfloat16)
+            part = pl.ds(pl.multiple_of(which * half + step * 16, 16), 16)
+            normed[part, :] = layer_norm(values[part, :], mix_gain[...], mix_shift[...]).astype(
+                jnp.bfloat16
+            )
 
     def route(which):
         where = halves[which]
@@ -368,14 +401,16 @@
     for which in (1, 0):
         where = halves[which]
         project(which)
-        rows_y[which] = send(normed.at[where], rows_in.at[0, where], to_y)
-        rows_z[which] = send(normed.at[where], rows_in.at[1, where], to_z)
         route(which)
         meta_y[which] = send(meta.at[which], meta_in.at[0, which], to_y)
         meta_z[which] = send(meta.at[which], meta_in.at[1, which], to_z)
+        rows_y[which] = send(normed.at[where], rows_in.at[0, where], to_y)
+        rows_z[which] = send(normed.at[where], rows_in.at[1, where], to_z)
+
+    start_far((6,), outer)
 
     slot_ids = lax.broadcasted_iota(jnp.int32, (slots, half), 0).astype(jnp.float32)
-    experts = (sp, flip(sp, group_size))
+    experts = (sp, opposite(sp))
 
     def select(position, which, row_ref, meta_ref):
         parts = []
@@ -391,7 +426,7 @@
         spread[position, which] = jnp.transpose(match).astype(jnp.bfloat16)
         match = match.astype(jnp.bfloat16)
 
-        @pl.loop(0, 4)
+        @pl.loop(0, 4, unroll=2)
         def _(step):
             wide = width // 4
             part = pl.ds(pl.multiple_of(step * wide, wide), wide)
@@ -403,31 +438,38 @@
                     kind * slots : (kind + 1) * slots
                 ]
 
-    def ffn(position, kind, gate, up, down):
-        @pl.loop(0, 2)
+    def activate(lines, gate, up):
+        gate_out = jnp.dot(lines, gate, preferred_element_type=jnp.float32)
+        up_out = jnp.dot(lines, up, preferred_element_type=jnp.float32)
+        return (gate_out / (1.0 + jnp.exp(-gate_out)) * up_out).astype(jnp.bfloat16)
+
+    def ffn(position, kind, gate, up, down, parts):
+        depth = parts * late
+
+        @pl.loop(0, parts)
         def _(step):
-            wide = ff // 2
-            part = pl.ds(pl.multiple_of(step * wide, wide), wide)
-            lines = picked[kind, position]
-            gate_out = jnp.dot(lines, gate[:, part], preferred_element_type=jnp.float32)
-            up_out = jnp.dot(lines, up[:, part], preferred_element_type=jnp.float32)
-            hidden[:, part] = (gate_out / (1.0 + jnp.exp(-gate_out)) * up_out).astype(jnp.bfloat16)
-
-        @pl.loop(0, 4)
+            part = pl.ds(pl.multiple_of(step * late, late), late)
+            hidden[:, part] = activate(picked[kind, position], gate[:, part], up[:, part])
+
+        @pl.loop(0, 4, unroll=2)
         def _(step):
             wide = width // 4
             part = pl.ds(pl.multiple_of(step * wide, wide), wide)
-            result = jnp.dot(hidden[...], down[:, part], preferred_element_type=jnp.float32)
+            result = jnp.dot(
+                hidden[:, :depth], down[:depth, part], preferred_element_type=jnp.float32
+            )
             result = (result * slot_weight[kind, position]).astype(jnp.bfloat16)
             for which in range(2):
                 weighted[position, which, pl.ds(kind * slots, slots), part] = result[
                     which * slots : (which + 1) * slots
                 ]
 
+    own, from_y, from_z, from_corner = 3, 0, 1, 2
+
     def gather_back(position):
         for which in range(2):
 
-            @pl.loop(0, 4)
+            @pl.loop(0, 4, unroll=2)
             def _(step):
                 wide = width // 4
                 part = pl.ds(pl.multiple_of(step * wide, wide), wide)
@@ -437,109 +479,279 @@
                     preferred_element_type=jnp.float32,
                 ).astype(jnp.bfloat16)
 
-    by_x, by_core, by_relay = [], [], []
+    def start_sum(which):
+        where = halves[which]
+
+        @pl.loop(0, 4, unroll=2)
+        def _(step):
+            wide = width // 4
+            part = pl.ds(pl.multiple_of(step * wide, wide), wide)
+            values[where, part] = skip_scale * normed[where, part].astype(jnp.float32) + jnp.dot(
+                spread[own, which], weighted[own, which, :, part], preferred_element_type=jnp.float32
+            )
 
     def pass_far(index):
-        own, kept, beside = chunks[index]
         far[index].wait_recv()
-        by_x.append(send(kept, kept, to_x))
-        by_core.append(send(kept, kept, to_core))
+        by_x[index].start()
+        by_core[index].start()
 
     def pass_x(index):
-        own, kept, beside = chunks[index]
         by_x[index].wait_recv()
-        by_relay.append(send(beside, beside, to_core))
-
-    own, from_y, from_z, from_corner = 3, 0, 1, 2
+        by_relay[index].start()
+
+    def settle(indices):
+        for index in indices:
+            by_core[index].wait_recv()
+            by_relay[index].wait_recv()
+
+    outermost = jnp.where(inner, flip(sp, 2), sp)
+    keepers = (outermost, flip(outermost, 1))
+    for which in range(2):
+        parts = []
+        for place, keeper in enumerate(keepers):
+            expert = opposite(keeper)
+            match = jnp.where(slot_ids == meta[which, pl.ds(expert, 1), :], 1.0, 0.0)
+            late_weight[place, pl.ds(which * slots, slots), :] = jnp.sum(
+                match * meta[which, pl.ds(expert_count + expert, 1), :], axis=1, keepdims=True
+            )
+            parts.append(match)
+        late_spread[which] = jnp.transpose(jnp.concatenate(parts, axis=0)).astype(jnp.bfloat16)
+
     select(own, 1, normed, meta)
     select(own, 0, normed, meta)
     for copy in experts_in:
         copy.wait()
-    ffn(own, 0, gate_a, up_a, down_a)
-    pass_far(0)
-
-    rows_y[1].wait_recv()
-    meta_y[1].wait_recv()
-    corner_1 = send(rows_in.at[0, second], rows_in.at[2, second], to_z)
-    corner_meta_1 = send(meta_in.at[0, 1], meta_in.at[2, 1], to_z)
-    for index in range(1, len(chunks)):
-        pl.when(jnp.logical_not(inner))(far[index].start)
-    select(from_y, 1, rows_in.at[0], meta_in.at[0])
-    rows_z[1].wait_recv()
-    meta_z[1].wait_recv()
-    select(from_z, 1, rows_in.at[1], meta_in.at[1])
-    pass_x(0)
-    rows_z[0].wait_recv()
-    meta_z[0].wait_recv()
-    corner_0 = send(rows_in.at[1, first], rows_in.at[2, first], to_y)
-    corner_meta_0 = send(meta_in.at[1, 0], meta_in.at[2, 0], to_y)
-    select(from_z, 0, rows_in.at[1], meta_in.at[1])
-    ffn(from_z, 0, gate_a, up_a, down_a)
-    rows_y[0].wait_recv()
-    meta_y[0].wait_recv()
-    select(from_y, 0, rows_in.at[0], meta_in.at[0])
-    ffn(from_y, 0, gate_a, up_a, down_a)
-    corner_1.wait_recv()
-    corner_meta_1.wait_recv()
-    select(from_corner, 1, rows_in.at[2], meta_in.at[2])
-    corner_0.wait_recv()
-    corner_meta_0.wait_recv()
-    select(from_corner, 0, rows_in.at[2], meta_in.at[2])
-    ffn(from_corner, 0, gate_a, up_a, down_a)
-    for index in range(1, len(chunks)):
-        pass_far(index)
-        if index > 1:
-            pass_x(index - 1)
-    pass_x(len(chunks) - 1)
-    for copy in by_core + by_relay:
-        copy.wait_recv()
-
-    ffn(from_corner, 1, gate_b, up_b, down_b)
-    gather_back(from_corner)
-    pass_y = send(partial.at[from_corner, first], passing.at[0], to_y)
-    pass_z = send(partial.at[from_corner, second], passing.at[1], to_z)
-    ffn(from_y, 1, gate_b, up_b, down_b)
-    gather_back(from_y)
-    back_y1 = send(partial.at[from_y, first], arrived.at[0, first], to_y)
-    ffn(from_z, 1, gate_b, up_b, down_b)
-    gather_back(from_z)
-    back_z2 = send(partial.at[from_z, second], arrived.at[1, second], to_z)
-
-    def add_passing(position, where, slot):
+    ffn(own, 0, gate_a, up_a, down_a, 2)
+
+    y_part, z_part = pl.ds(0, back_y), pl.ds(back_y, rows - back_y)
+    corner_meta_1 = send(meta_in.at[0, 1], meta_in.at[2, 1], to_z, start=False)
+    corner_meta_0 = send(meta_in.at[1, 0], meta_in.at[2, 0], to_y, start=False)
+    corner_1 = send(rows_in.at[1, second], rows_in.at[2, second], to_y, start=False)
+    corner_0 = send(rows_in.at[1, first], rows_in.at[2, first], to_y, start=False)
+    late_z = send(late_a.at[:, mine], late_a.at[:, mine], to_z, outer, start=False)
+    late_y = send(late_a.at[:, mine], late_b.at[:, mine], to_y, start=False)
+    late_x = send(late_b.at[:, mine], late_b.at[:, mine], to_x, start=False)
+    late_core = send(late_b.at[:, mine], late_b.at[:, mine], to_core, start=False)
+    late_relay = send(late_b.at[:, across], late_b.at[:, across], to_core, start=False)
+    pass_y = send(partial.at[from_corner, y_part], passing.at[y_part], to_y, start=False)
+    pass_z = send(partial.at[from_corner, z_part], passing.at[z_part], to_z, start=False)
+    back_y1 = send(partial.at[from_y, y_part], arrived.at[0, y_part], to_y, start=False)
+    back_z1 = send(partial.at[from_z, z_part], arrived.at[1, z_part], to_z, start=False)
+    back_y2 = send(partial.at[from_y, z_part], arrived.at[0, z_part], to_y, start=False)
+    back_z2 = send(partial.at[from_z, y_part], arrived.at[1, y_part], to_z, start=False)
+    hidden_y = send(hidden_out.at[0], hidden_in.at[1], to_y, outer, start=False)
+    hidden_z = send(hidden_out.at[1], hidden_in.at[0], to_z, outer, start=False)
+    hidden_corner = send(hidden_out.at[2], hidden_in.at[1], to_corner, outer, start=False)
+
+    def take_y1():
+        meta_y[1].wait_recv()
+        corner_meta_1.start()
+        rows_y[1].wait_recv()
+        select(from_y, 1, rows_in.at[0], meta_in.at[0])
+
+    def take_y0():
+        meta_y[0].wait_recv()
+        rows_y[0].wait_recv()
+        select(from_y, 0, rows_in.at[0], meta_in.at[0])
+        ffn(from_y, 0, gate_a, up_a, down_a, 2)
+
+    def take_z1():
+        meta_z[1].wait_recv()
+        rows_z[1].wait_recv()
+        corner_1.start()
+        select(from_z, 1, rows_in.at[1], meta_in.at[1])
+
+    def take_z0():
+        meta_z[0].wait_recv()
+        corner_meta_0.start()
+        rows_z[0].wait_recv()
+        corner_0.start()
+        select(from_z, 0, rows_in.at[1], meta_in.at[1])
+        ffn(from_z, 0, gate_a, up_a, down_a, 2)
+
+    def take_corner1():
+        corner_meta_1.wait_recv()
+        corner_1.wait_recv()
+        select(from_corner, 1, rows_in.at[2], meta_in.at[2])
+
+    def take_corner0():
+        corner_meta_0.wait_recv()
+        corner_0.wait_recv()
+        select(from_corner, 0, rows_in.at[2], meta_in.at[2])
+        ffn(from_corner, 0, gate_a, up_a, down_a, 2)
+
+    def start_late():
+        late_y.start()
+        by_x[6].start()
+        by_core[6].start()
+
+    def pass_late():
+        late_y.wait_recv()
+        late_x.start()
+        late_core.start()
+
+    def relay_late():
+        late_x.wait_recv()
+        late_relay.start()
+
+    def add_passing(position, where):
         partial[position, where, :] = (
-            partial[position, where, :].astype(jnp.float32) + passing[slot].astype(jnp.float32)
+            partial[position, where, :].astype(jnp.float32) + passing[where].astype(jnp.float32)
         ).astype(jnp.bfloat16)
 
-    ffn(own, 1, gate_b, up_b, down_b)
-    pass_y.wait_recv()
-    add_passing(from_z, first, 0)
-    back_z1 = send(partial.at[from_z, first], arrived.at[1, first], to_z)
-    pass_z.wait_recv()
-    add_passing(from_y, second, 1)
-    back_y2 = send(partial.at[from_y, second], arrived.at[0, second], to_y)
+    def merge_z():
+        pass_z.wait_recv()
+        add_passing(from_y, z_part)
+        back_y2.start()
+
+    def merge_y():
+        pass_y.wait_recv()
+        add_passing(from_z, y_part)
+        back_z2.start()
+
+    def finish(position, parts, *copies):
+        ffn(position, 1, gate_b, up_b, down_b, parts)
+        gather_back(position)
+        for copy in copies:
+            copy.start()
+
+    def finish_own(parts):
+        ffn(own, 1, gate_b, up_b, down_b, parts)
+        for which in range(2):
+            start_sum(which)
+
+    def late_hidden(position, place, copy):
+        lines = activate(picked[1, position], gate_b[:, later], up_b[:, later])
+        if copy is None:
+            hidden_in[place] = lines
+        else:
+            hidden_out[place] = lines
+            copy.start()
+
+    def add_late(which):
+        @pl.loop(0, 4, unroll=2)
+        def _(step):
+            wide = width // 4
+            part = pl.ds(pl.multiple_of(step * wide, wide), wide)
+            values[halves[which], part] += jnp.dot(
+                late_spread[which], late_rows[which, :, part], preferred_element_type=jnp.float32
+            )
+
+    def late_result(place, down):
+        @pl.loop(0, 4, unroll=2)
+        def _(step):
+            wide = width // 4
+            part = pl.ds(pl.multiple_of(step * wide, wide), wide)
+            result = jnp.dot(hidden_in[place], down[:, part], preferred_element_type=jnp.float32)
+            result = (result * late_weight[place]).astype(jnp.bfloat16)
+            for which in range(2):
+                late_rows[which, pl.ds(place * slots, slots), part] = result[
+                    which * slots : (which + 1) * slots
+                ]
+
+    @pl.when(outer)
+    def _():
+        pass_far(0)
+        pass_far(1)
+        take_y1()
+        pass_far(2)
+        pass_x(0)
+        pass_x(1)
+        take_z1()
+        pass_x(2)
+        take_y0()
+        settle((0, 1, 2))
+        take_z0()
+        finish(from_z, 1)
+        far[6].wait_recv()
+        late_z.start()
+        start_late()
+        finish(from_y, 1, back_y1)
+        take_corner1()
+        pass_x(6)
+        take_corner0()
+        start_far((3, 4), outer)
+        back_z1.start()
+        finish(from_corner, 1, pass_y, pass_z)
+        finish_own(1)
+        pass_late()
+        pass_far(3)
+        relay_late()
+        pass_far(4)
+        pass_x(3)
+        merge_z()
+        pass_x(4)
+        settle((3, 4))
+        late_hidden(from_corner, 2, hidden_corner)
+        late_hidden(from_y, 0, hidden_y)
+        late_hidden(from_z, 1, hidden_z)
+        merge_y()
+        late_hidden(own, 0, None)
+        settle((6,))
+        late_core.wait_recv()
+        late_relay.wait_recv()
+        late_result(0, late_a)
+        hidden_y.wait_recv()
+
+    @pl.when(inner)
+    def _():
+        take_y1()
+        pass_far(0)
+        take_z1()
+        pass_far(1)
+        pass_x(0)
+        take_y0()
+        pass_far(2)
+        pass_x(1)
+        take_z0()
+        pass_far(3)
+        pass_x(2)
+        pass_far(4)
+        pass_x(3)
+        take_corner1()
+        pass_far(5)
+        pass_x(4)
+        take_corner0()
+        late_z.wait_recv()
+        start_late()
+        pass_x(5)
+        settle((0, 1, 2, 3, 4, 5))
+        finish(from_corner, 2, pass_y, pass_z)
+        finish(from_y, 2, back_y1)
+        finish(from_z, 2, back_z1)
+        pass_x(6)
+        finish_own(2)
+        pass_late()
+        merge_z()
+        relay_late()
+        merge_y()
+        settle((6,))
+        late_core.wait_recv()
+        late_relay.wait_recv()
+        hidden_z.wait_recv()
+        late_result(0, late_a)
+        hidden_corner.wait_recv()
+
+    late_result(1, late_b)
+    for which in range(2):
+        add_late(which)
     for copy in ends:
         copy.wait()
-    for copy in (back_y1, back_z2, back_z1, back_y2):
+    for copy in (back_y1, back_z1, back_y2, back_z2):
         copy.wait_recv()
 
-    for which in range(2):
-
-        @pl.loop(0, half // 64)
-        def _(step):
-            inside = pl.ds(pl.multiple_of(step * 64, 64), 64)
-            part = pl.ds(pl.multiple_of(which * half + step * 64, 64), 64)
-            routed = jnp.dot(
-                spread[own, which, inside, :],
-                weighted[own, which],
-                preferred_element_type=jnp.float32,
-            )
-            routed = routed + arrived[0, part, :].astype(jnp.float32)
-            routed = routed + arrived[1, part, :].astype(jnp.float32)
-            total = skip_scale * normed[part, :].astype(jnp.float32) + routed
-            out[part, :] = layer_norm(total, gain[...], shift[...]).astype(jnp.bfloat16)
-
-    for copy in made:
-        copy.wait_send()
+    @pl.loop(0, rows // 16, unroll=2)
+    def _(step):
+        part = pl.ds(pl.multiple_of(step * 16, 16), 16)
+        total = values[part, :] + arrived[0, part, :].astype(jnp.float32)
+        total = total + arrived[1, part, :].astype(jnp.float32)
+        out[part, :] = layer_norm(total, gain[...], shift[...]).astype(jnp.bfloat16)
+
+    for copy, when in made:
+        if when is None:
+            copy.wait_send()
+        else:
+            pl.when(when)(copy.wait_send)
 
 
 def near_layer(
@@ -609,7 +821,7 @@
             pltpu.VMEM((1, width), f32),
             pltpu.VMEM((6, block, group_width), bf16),
             pltpu.VMEM((2, half, pool_width), bf16),
-            pltpu.VMEM((half, width), f32),
+            pltpu.VMEM((rows, width), f32),
             pltpu.VMEM((rows, width), bf16),
             pltpu.VMEM((2, 2 * expert_count, half), f32),
             pltpu.VMEM((width, ff), bf16),
@@ -626,11 +838,18 @@
             pltpu.VMEM((2 * slots, ff), bf16),
             pltpu.VMEM((4, 2, 2 * slots, width), bf16),
             pltpu.VMEM((3, rows, width), bf16),
-            pltpu.VMEM((2, half, width), bf16),
+            pltpu.VMEM((rows, width), bf16),
             pltpu.VMEM((2, rows, width), bf16),
+            pltpu.VMEM((3, 2 * slots, ff // 2), bf16),
+            pltpu.VMEM((2, 2 * slots, ff // 2), bf16),
+            pltpu.VMEM((ff // 2, width), bf16),
+            pltpu.VMEM((ff // 2, width), bf16),
+            pltpu.VMEM((2, half, 2 * slots), bf16),
+            pltpu.VMEM((2, 2 * slots, 1), f32),
+            pltpu.VMEM((2, 2 * slots, width), bf16),
             pltpu.SemaphoreType.DMA((16,)),
-            pltpu.SemaphoreType.DMA((64,)),
-            pltpu.SemaphoreType.DMA((64,)),
+            pltpu.SemaphoreType.DMA((80,)),
+            pltpu.SemaphoreType.DMA((80,)),
         ],
         compiler_params=pltpu.CompilerParams(
             collective_id=0, has_side_effects=True, vmem_limit_bytes=60 * 1024 * 1024

time: 161 us -> 119 us (0.74)
  Pallas kernels: 158 us -> 117 us
    pallas_call x1, Pallas kernels: 158 us -> 117 us  [near_layer(): pl.pallas_call(functools.partial(layer_kernel, (slots, expert_count)), ou...]
where the time goes in v2:
time: 119 us
  Pallas kernels  117 us (98%)
  local copies, waits for them, and re-layouts  2.3 us (2%)
    pallas_call x1, Pallas kernels, near_layer(): pl.pallas_call(functools.partial(layer_kernel, (slots, expert_count)), ou...  117 us

profile of v2, /device:TPU:0, one launch (start us, length us, event | category | flops | bytes accessed | tf_op | source)
XLA Modules:
  0.0 119.0 jit_solution(9629873379478342672)
XLA Ops:
  0.0 116.7 %shard_map.154 = bf16[256,2048]{1,0:T(8,128)(2,1)} custom-call(bf16[256,2048]{1,0:T(8,128)(2,1)} %residual_hbm.1, bf16[1024,256]{1,0:T(8,128)(2,1)} %pool_hbm.1, s32[8,128]{1,0:T(8,128)} %bitcast.15, bf16[1,256,256]{2,1,0:T(8,128)(2,1)} %map_hbm.1, f32[1,256]{1,0:T(1,128)} %bitcast.17, bf16[1024,2048]{1,0:T(8,128)(2,1)} %weight_hbm.1, f32[1,2048]{1,0:T(1,128)} %bitcast.11, ...), custom_call_target="tpu_custom_call" | custom-call | tf_op jit(solution)/shard_map/pallas_call | solution.py:803
  116.7 2.3 %copy.18 = bf16[256,2048]{1,0:T(8,128)(2,1)} copy(bf16[256,2048]{1,0:T(8,128)(2,1)} %shard_map.154) | data formatting | bytes 2097152

commit v3 on v2

--- a/solution.py
+++ b/solution.py
@@ -168,7 +168,7 @@
     ff = own_gate.shape[2]
     seq_rows, group_width = pool_hbm.shape
     reach = 16
-    back_y = rows // 2
+    outer_y, inner_y = rows * 13 // 16, rows // 2
     sp, tp = lax.axis_index("sp"), lax.axis_index("tp")
     sp_count = expert_count
     to_y = {"sp": flip(sp, 1)}
@@ -523,7 +523,6 @@
         copy.wait()
     ffn(own, 0, gate_a, up_a, down_a, 2)
 
-    y_part, z_part = pl.ds(0, back_y), pl.ds(back_y, rows - back_y)
     corner_meta_1 = send(meta_in.at[0, 1], meta_in.at[2, 1], to_z, start=False)
     corner_meta_0 = send(meta_in.at[1, 0], meta_in.at[2, 0], to_y, start=False)
     corner_1 = send(rows_in.at[1, second], rows_in.at[2, second], to_y, start=False)
@@ -533,12 +532,29 @@
     late_x = send(late_b.at[:, mine], late_b.at[:, mine], to_x, start=False)
     late_core = send(late_b.at[:, mine], late_b.at[:, mine], to_core, start=False)
     late_relay = send(late_b.at[:, across], late_b.at[:, across], to_core, start=False)
-    pass_y = send(partial.at[from_corner, y_part], passing.at[y_part], to_y, start=False)
-    pass_z = send(partial.at[from_corner, z_part], passing.at[z_part], to_z, start=False)
-    back_y1 = send(partial.at[from_y, y_part], arrived.at[0, y_part], to_y, start=False)
-    back_z1 = send(partial.at[from_z, z_part], arrived.at[1, z_part], to_z, start=False)
-    back_y2 = send(partial.at[from_y, z_part], arrived.at[0, z_part], to_y, start=False)
-    back_z2 = send(partial.at[from_z, y_part], arrived.at[1, y_part], to_z, start=False)
+
+    def split(count):
+        return pl.ds(0, count), pl.ds(count, rows - count)
+
+    def results(plane, mine_y, other_y):
+        def move(position, where, place, slot, peer):
+            return send(
+                partial.at[position, where], place.at[slot, where], peer, plane, start=False
+            )
+
+        y_part, z_part = split(mine_y)
+        first_part, last_part = split(other_y)
+        return (
+            move(from_corner, y_part, passing, 0, to_y),
+            move(from_corner, z_part, passing, 1, to_z),
+            move(from_y, first_part, arrived, 0, to_y),
+            move(from_y, last_part, arrived, 0, to_y),
+            move(from_z, z_part, arrived, 1, to_z),
+            move(from_z, y_part, arrived, 1, to_z),
+        )
+
+    outer_results = results(outer, outer_y, inner_y)
+    inner_results = results(inner, inner_y, outer_y)
     hidden_y = send(hidden_out.at[0], hidden_in.at[1], to_y, outer, start=False)
     hidden_z = send(hidden_out.at[1], hidden_in.at[0], to_z, outer, start=False)
     hidden_corner = send(hidden_out.at[2], hidden_in.at[1], to_corner, outer, start=False)
@@ -594,20 +610,21 @@
         late_x.wait_recv()
         late_relay.start()
 
-    def add_passing(position, where):
+    def add_passing(position, where, slot):
         partial[position, where, :] = (
-            partial[position, where, :].astype(jnp.float32) + passing[where].astype(jnp.float32)
+            partial[position, where, :].astype(jnp.float32)
+            + passing[slot, where, :].astype(jnp.float32)
         ).astype(jnp.bfloat16)
 
-    def merge_z():
-        pass_z.wait_recv()
-        add_passing(from_y, z_part)
-        back_y2.start()
-
-    def merge_y():
-        pass_y.wait_recv()
-        add_passing(from_z, y_part)
-        back_z2.start()
+    def merge_z(here, there, other_y):
+        there[1].wait_recv()
+        add_passing(from_y, split(other_y)[1], 1)
+        here[3].start()
+
+    def merge_y(here, mine_y):
+        here[0].wait_recv()
+        add_passing(from_z, split(mine_y)[0], 0)
+        here[5].start()
 
     def finish(position, parts, *copies):
         ffn(position, 1, gate_b, up_b, down_b, parts)
@@ -651,6 +668,7 @@
 
     @pl.when(outer)
     def _():
+        pass_y, pass_z, back_y1, back_y2, back_z1, back_z2 = outer_results
         pass_far(0)
         pass_far(1)
         take_y1()
@@ -666,26 +684,26 @@
         far[6].wait_recv()
         late_z.start()
         start_late()
-        finish(from_y, 1, back_y1)
+        back_z1.start()
+        finish(from_y, 1)
         take_corner1()
         pass_x(6)
         take_corner0()
         start_far((3, 4), outer)
-        back_z1.start()
-        finish(from_corner, 1, pass_y, pass_z)
+        finish(from_corner, 1, pass_y, pass_z, back_y1)
         finish_own(1)
         pass_late()
         pass_far(3)
         relay_late()
         pass_far(4)
         pass_x(3)
-        merge_z()
         pass_x(4)
         settle((3, 4))
         late_hidden(from_corner, 2, hidden_corner)
         late_hidden(from_y, 0, hidden_y)
         late_hidden(from_z, 1, hidden_z)
-        merge_y()
+        merge_y(outer_results, outer_y)
+        merge_z(outer_results, inner_results, inner_y)
         late_hidden(own, 0, None)
         settle((6,))
         late_core.wait_recv()
@@ -695,6 +713,7 @@
 
     @pl.when(inner)
     def _():
+        pass_y, pass_z, back_y1, back_y2, back_z1, back_z2 = inner_results
         take_y1()
         pass_far(0)
         take_z1()
@@ -713,8 +732,10 @@
         pass_x(4)
         take_corner0()
         late_z.wait_recv()
-        start_late()
+        late_y.start()
         pass_x(5)
+        by_x[6].start()
+        by_core[6].start()
         settle((0, 1, 2, 3, 4, 5))
         finish(from_corner, 2, pass_y, pass_z)
         finish(from_y, 2, back_y1)
@@ -722,9 +743,9 @@
         pass_x(6)
         finish_own(2)
         pass_late()
-        merge_z()
+        merge_y(inner_results, inner_y)
+        merge_z(inner_results, outer_results, outer_y)
         relay_late()
-        merge_y()
         settle((6,))
         late_core.wait_recv()
         late_relay.wait_recv()
@@ -737,10 +758,23 @@
         add_late(which)
     for copy in ends:
         copy.wait()
-    for copy in (back_y1, back_z1, back_y2, back_z2):
-        copy.wait_recv()
-
-    @pl.loop(0, rows // 16, unroll=2)
+
+    @pl.when(outer)
+    def _():
+        outer_results[2].wait_recv()
+        outer_results[3].wait_recv()
+        inner_results[4].wait_recv()
+        inner_results[5].wait_recv()
+
+    @pl.when(inner)
+    def _():
+        inner_results[2].wait_recv()
+        inner_results[3].wait_recv()
+        outer_results[4].wait_recv()
+        outer_results[5].wait_recv()
+
+
+    @pl.loop(0, rows // 16, unroll=4)
     def _(step):
         part = pl.ds(pl.multiple_of(step * 16, 16), 16)
         total = values[part, :] + arrived[0, part, :].astype(jnp.float32)
@@ -838,7 +872,7 @@
             pltpu.VMEM((2 * slots, ff), bf16),
             pltpu.VMEM((4, 2, 2 * slots, width), bf16),
             pltpu.VMEM((3, rows, width), bf16),
-            pltpu.VMEM((rows, width), bf16),
+            pltpu.VMEM((2, rows, width), bf16),
             pltpu.VMEM((2, rows, width), bf16),
             pltpu.VMEM((3, 2 * slots, ff // 2), bf16),
             pltpu.VMEM((2, 2 * slots, ff // 2), bf16),

time: 119 us -> 118 us (level)
  no operation moved by 1% of the time
where the time goes in v3:
time: 118 us
  Pallas kernels  116 us (98%)
  local copies, waits for them, and re-layouts  2.3 us (2%)
    pallas_call x1, Pallas kernels, near_layer(): pl.pallas_call(functools.partial(layer_kernel, (slots, expert_count)), ou...  116 us

profile of v3, /device:TPU:0, one launch (start us, length us, event | category | flops | bytes accessed | tf_op | source)
XLA Modules:
  0.0 118.1 jit_solution(3254443605061555595)
XLA Ops:
  0.0 115.8 %shard_map.154 = bf16[256,2048]{1,0:T(8,128)(2,1)} custom-call(bf16[256,2048]{1,0:T(8,128)(2,1)} %residual_hbm.1, bf16[1024,256]{1,0:T(8,128)(2,1)} %pool_hbm.1, s32[8,128]{1,0:T(8,128)} %bitcast.15, bf16[1,256,256]{2,1,0:T(8,128)(2,1)} %map_hbm.1, f32[1,256]{1,0:T(1,128)} %bitcast.17, bf16[1024,2048]{1,0:T(8,128)(2,1)} %weight_hbm.1, f32[1,2048]{1,0:T(1,128)} %bitcast.11, ...), custom_call_target="tpu_custom_call" | custom-call | tf_op jit(solution)/shard_map/pallas_call | solution.py:837
  115.8 2.3 %copy.18 = bf16[256,2048]{1,0:T(8,128)(2,1)} copy(bf16[256,2048]{1,0:T(8,128)(2,1)} %shard_map.154) | data formatting | bytes 2097152
